TPU v7x, 512 devices: a whole 4x4x16 slice. The times are simulated.
512 devices in a mesh: sp: 64 (over z, y), tp: 8 (over x, core).
Axes of the slice: x: 4, y: 4, z: 16, core: 2. Of those that a mesh axis runs over, the one named last changes fastest.
Arguments:
- tokens: bfloat16 [16384, 2048], P(('sp', 'tp')), may hold values from -6 to 6
- norm_gain: float32 [2048], replicated, may hold values from 0.1 to 1.9
- recept_weight: bfloat16 [2048, 1024], P(None, 'tp'), may hold values from -0.125 to 0.125
- key_weight: bfloat16 [2048, 1024], P(None, 'tp'), may hold values from -0.125 to 0.125
- value_weight: bfloat16 [2048, 1024], P(None, 'tp'), may hold values from -0.125 to 0.125
- decay_down_weight: bfloat16 [2048, 64], replicated, may hold values from -0.125 to 0.125
- rate_down: bfloat16 [2048, 64], replicated, may hold values from -0.125 to 0.125
- decay_up: bfloat16 [64, 1024], P(None, 'tp'), may hold values from -0.75 to 0.75
- rate_up: bfloat16 [64, 1024], P(None, 'tp'), may hold values from -0.75 to 0.75
- decay_base: float32 [1024], P('tp'), may hold values from -16 to -3
- rate_base: float32 [1024], P('tp'), may hold values from -12 to 1
- decay_extra: float32 [16384, 16], P('sp', 'tp'), may hold values from -3 to 0
- group_gain: float32 [1024], P('tp'), may hold values from 0.1 to 1.9
- attn_query: bfloat16 [2048, 1024], P(None, 'tp'), may hold values from -0.125 to 0.125
- attn_key: bfloat16 [2048, 1024], P(None, 'tp'), may hold values from -0.125 to 0.125
- attn_value: bfloat16 [2048, 1024], P(None, 'tp'), may hold values from -0.125 to 0.125
- query_gain: float32 [64], replicated, may hold values from 1 to 9
- key_gain: float32 [64], replicated, may hold values from 1 to 9
- lambdas: float32 [8], P('tp'), may hold values from 0.3 to 0.8
- head_gain: float32 [128], replicated, may hold values from 0.1 to 1.9
- out_linear: bfloat16 [1024, 2048], P('tp'), may hold values from -0.15625 to 0.15625
- out_attn: bfloat16 [1024, 2048], P('tp'), may hold values from -0.1875 to 0.1875
Outputs:
- mixed: bfloat16 [16384, 2048], P(('sp', 'tp'))
All inputs are finite; a program needn't handle non-finite values.
Results may differ from a plain program's by a relative error of at most 0.018.
The roundings to bfloat16 on the way count: a program that leaves them out, or rounds other values in their place, can miss the bound.
Values may be sent and summed in bfloat16 or wider, within the bound.
No kernel may reach another device: no remote copies, remote signals or barrier semaphores. Data moves between devices by JAX's collectives and lax.ppermute only.
A program may use at most 128 MiB of HBM per device.

v0:
```python
import jax
import jax.numpy as jnp
from jax import lax
from jax.sharding import Mesh
from jax.sharding import PartitionSpec as P

LINEAR_HEAD_WIDTH = 64
HEAD_C = 64
BLOCK_A = 64
SP = ("sp_0", "sp_1")
SP_TP = ("sp_0", "sp_1", "tp")


group_eps = 0.00064
norm_eps = 1e-06
key_span = 1024


def copy_for_each(x, axis):
    copies = jnp.broadcast_to(x, (lax.axis_size(axis), *x.shape))
    return lax.all_to_all(copies, axis, split_axis=0, concat_axis=0, tiled=True)


def in_order(blocks, dim):
    dims = list(blocks.shape[1:])
    dims[dim] *= blocks.shape[0]
    return jnp.moveaxis(blocks, 0, dim).reshape(dims)


def collect(x, axis, dim):
    blocks = copy_for_each(x, axis)
    return in_order(blocks, dim)


def filled_with(x, identity):
    return jnp.broadcast_to(jnp.asarray(identity, x.dtype), x.shape)


def prefix_by_axis(x, axes, combine, identity):
    before = start = filled_with(x, identity)
    subtotal = x
    for axis in reversed(axes):
        peers, position = (lax.axis_size(axis), lax.axis_index(axis))
        pieces = lax.all_gather(subtotal, axis)
        inside, subtotal = (start, start)
        for k in range(peers):
            passed = k < position
            subtotal = combine(subtotal, pieces[k])
            inside = jnp.where(passed, subtotal, inside)
        before = combine(inside, before)
    return before


def side_by_side(arrays, axis, dim, along):
    widths = [a.shape[along] for a in arrays]
    both = jnp.concatenate(arrays, axis=along)
    whole = lax.all_gather(both, axis, axis=dim, tiled=True)
    return tuple(jnp.split(whole, [sum(widths[:k]) for k in range(1, len(widths))], axis=along))


def in_blocks(x, dim, peers):
    dims = x.shape
    blocks = x.reshape(*dims[:dim], peers, dims[dim] // peers, *dims[dim + 1 :])
    return jnp.moveaxis(blocks, dim, 0)


def sum_at_owner(x, axis, dim):
    blocks = in_blocks(x, dim, lax.axis_size(axis))
    arrived = lax.all_to_all(blocks, axis, split_axis=0, concat_axis=0, tiled=True)
    return arrived.astype(jnp.float32).sum(axis=0)


def rms_scale(values, gain):
    return values * lax.rsqrt(jnp.mean(values * values, -1, keepdims=True) + norm_eps) * gain


def batched_rows(left, right):
    return jnp.einsum("hij,hjr->hir", left, right)


def ratio_dots(left, right, ratios):
    return jnp.einsum("hin,hjn,hijn->hij", left, right, ratios)


def unit_lower_inverse(lower):
    extent = lower.shape[-1]
    power_term = lower
    result = jnp.eye(extent, dtype=jnp.float32) + lower
    for repeat_turn in range((extent - 1).bit_length() - 1):
        power_term = batched_rows(power_term, power_term)
        result = result + batched_rows(result, power_term)
    return result


def block_step(memory, inputs):
    recept, log_step, remove, restore, values, inject = inputs
    extent = recept.shape[1]
    row_index = jnp.arange(extent)[:, None]
    col_index = jnp.arange(extent)[None, :]
    lower_incl = row_index >= col_index
    strict = row_index > col_index
    cumulative = jnp.einsum("ij,hjn->hin", lower_incl.astype(jnp.float32), log_step)
    previous = cumulative - log_step
    closing = cumulative[:, -1:, :]
    spread = cumulative[:, :, None, :] - cumulative[:, None, :, :]
    ratio_incl = jnp.exp(jnp.where(lower_incl[None, :, :, None], spread, -jnp.inf))
    ratio_strict = jnp.exp(
        jnp.where(strict[None, :, :, None], spread - log_step[:, :, None, :], -jnp.inf)
    )
    remove_dec = remove * jnp.exp(previous)
    recept_dec = recept * jnp.exp(cumulative)
    restore_end = restore * jnp.exp(closing - cumulative)
    inject_end = inject * jnp.exp(closing - cumulative)
    full_values = jnp.concatenate([jnp.zeros_like(values), values], axis=-1)
    low_restore = ratio_dots(remove, restore, ratio_strict)
    low_inject = ratio_dots(remove, inject, ratio_strict)
    out_restore = ratio_dots(recept, restore, ratio_incl)
    out_inject = ratio_dots(recept, inject, ratio_incl)
    along = batched_rows(
        unit_lower_inverse(low_restore),
        batched_rows(remove_dec, memory) + batched_rows(low_inject, full_values),
    )
    result = (
        batched_rows(recept_dec, memory)
        + batched_rows(out_restore, along)
        + batched_rows(out_inject, full_values)
    )
    memory = (
        jnp.exp(closing)[:, 0, :, None] * memory
        + jnp.einsum("hcn,hcr->hnr", restore_end, along)
        + jnp.einsum("hcn,hcr->hnr", inject_end, full_values)
    )
    return (memory, result)


def chain_combine(earlier, later):
    extent = later.shape[-2]
    moved = jnp.einsum("...ij,...jr->...ir", later[..., :extent], earlier)
    kept = jnp.concatenate([jnp.zeros_like(later[..., :extent]), later[..., extent:]], axis=-1)
    return moved + kept


def shards(
    tokens,
    norm_gain,
    recept_weight,
    key_weight,
    value_weight,
    decay_down_weight,
    rate_down,
    decay_up,
    rate_up,
    decay_base,
    rate_base,
    decay_extra,
    group_gain,
    attn_query,
    attn_key,
    attn_value,
    query_gain,
    key_gain,
    lambdas,
    head_gain,
    out_linear,
    out_attn,
):
    normed = rms_scale(tokens.astype(jnp.float32), norm_gain).astype(jnp.bfloat16)
    width_a = recept_weight.shape[1]
    width_c = attn_query.shape[1]
    low_width = decay_down_weight.shape[1]
    joined = jnp.concatenate(
        [
            recept_weight,
            key_weight,
            value_weight,
            decay_down_weight,
            rate_down,
            attn_query,
            attn_key,
            attn_value,
        ],
        axis=1,
    )
    projected = jnp.dot(
        collect(normed, "tp", 0), joined, preferred_element_type=jnp.float32
    ).astype(jnp.bfloat16)
    length = projected.shape[0]
    widths = [width_a, width_a, width_a, low_width, low_width, width_c, width_c, width_c]
    sections = []
    offset = 0
    for extent in widths:
        sections.append(projected[:, offset : offset + extent])
        offset = offset + extent
    recept_b, lin_key_b, lin_value_b, decay_low, rate_low, query_b, key_b, values_c = sections
    heads_a = width_a // LINEAR_HEAD_WIDTH

    def split_heads(values):
        return values.astype(jnp.float32).reshape(length, heads_a, LINEAR_HEAD_WIDTH)

    recept = split_heads(recept_b)
    lin_key = split_heads(lin_key_b)
    lin_value = split_heads(lin_value_b)
    decay_mix = jnp.dot(decay_low, decay_up, preferred_element_type=jnp.float32)
    rate_mix = jnp.dot(rate_low, rate_up, preferred_element_type=jnp.float32)
    log_decay = split_heads(-jnp.exp(decay_base + jnp.tanh(decay_mix))) + decay_extra[:, :, None]
    rate_gate = split_heads(jax.nn.sigmoid(rate_base + jnp.tanh(rate_mix)))
    unit_key = lin_key * lax.rsqrt(jnp.sum(lin_key * lin_key, -1, keepdims=True) + norm_eps)
    remove = -unit_key
    restore = unit_key * rate_gate
    inject = lin_key * rate_gate

    def to_blocks(values):
        return values.reshape(length // BLOCK_A, BLOCK_A, heads_a, LINEAR_HEAD_WIDTH).transpose(
            0, 2, 1, 3
        )

    identity = jnp.concatenate(
        [
            jnp.broadcast_to(
                jnp.eye(LINEAR_HEAD_WIDTH, dtype=jnp.float32),
                (heads_a, LINEAR_HEAD_WIDTH, LINEAR_HEAD_WIDTH),
            ),
            jnp.zeros((heads_a, LINEAR_HEAD_WIDTH, LINEAR_HEAD_WIDTH), jnp.float32),
        ],
        axis=-1,
    )
    final_state, result_list = lax.scan(
        block_step,
        identity,
        tuple(
            (to_blocks(item) for item in (recept, log_decay, remove, restore, lin_value, inject))
        ),
    )
    result_list = result_list.transpose(0, 2, 1, 3).reshape(length, heads_a, 2 * LINEAR_HEAD_WIDTH)
    position = lax.axis_index(SP)
    before = prefix_by_axis(final_state, SP, chain_combine, identity)
    carried_state = before[..., LINEAR_HEAD_WIDTH:]
    read_out = result_list[..., LINEAR_HEAD_WIDTH:] + jnp.einsum(
        "leb,ebr->ler", result_list[..., :LINEAR_HEAD_WIDTH], carried_state
    )
    head_mean = jnp.mean(read_out, -1, keepdims=True)
    centered = read_out - head_mean
    head_var = jnp.mean(centered * centered, -1, keepdims=True)
    linear_part = (
        centered * lax.rsqrt(head_var + group_eps) * group_gain.reshape(heads_a, LINEAR_HEAD_WIDTH)
    )
    linear_part = linear_part.reshape(length, width_a).astype(jnp.bfloat16)
    heads_c = lambdas.shape[0]
    queries = rms_scale(
        query_b.astype(jnp.float32).reshape(length, heads_c, 2, HEAD_C), query_gain
    ).astype(jnp.bfloat16)
    keys_normed = (
        rms_scale(key_b.astype(jnp.float32).reshape(length, heads_c, 2, HEAD_C), key_gain)
        .astype(jnp.bfloat16)
        .reshape(length, width_c)
    )
    score_scale = HEAD_C ** (-0.5)
    query_pos = position * length + jnp.arange(length)
    query_last = position * length + length - 1

    def block_scores(key_rows, offset):
        key_heads = key_rows.reshape(key_rows.shape[0], heads_c, 2, HEAD_C)
        scores = (
            jnp.einsum("qhmd,khmd->hmqk", queries, key_heads, preferred_element_type=jnp.float32)
            * score_scale
        )
        key_pos = offset + jnp.arange(key_rows.shape[0])
        allowed = key_pos[None, :] <= query_pos[:, None]
        return jnp.where(allowed, scores, -jnp.inf)

    def add_stats(row_stats, key_rows, offset):
        row_top, row_sum = row_stats
        scores = block_scores(key_rows, offset)
        new_top = jnp.maximum(row_top, jnp.max(scores, -1))
        row_sum = row_sum * jnp.exp(row_top - new_top) + jnp.sum(
            jnp.exp(scores - new_top[..., None]), -1
        )
        return (new_top, row_sum)

    def add_values(accumulated, key_rows, value_rows, offset, row_stats):
        row_top, row_sum = row_stats
        scores = block_scores(key_rows, offset)
        probability = jnp.exp(scores - row_top[..., None]) / row_sum[..., None]
        weights = (probability[:, 0] - lambdas[:, None, None] * probability[:, 1]).astype(
            jnp.bfloat16
        )
        value_heads = value_rows.reshape(value_rows.shape[0], heads_c, 2 * HEAD_C)
        return accumulated + jnp.einsum(
            "hqk,khe->qhe", weights, value_heads, preferred_element_type=jnp.float32
        )

    start_stats = (
        jnp.full((heads_c, 2, length), -1e30, jnp.float32),
        jnp.zeros((heads_c, 2, length), jnp.float32),
    )
    start_values = jnp.zeros((length, heads_c, 2 * HEAD_C), jnp.float32)
    all_keys, all_values = side_by_side((keys_normed, values_c), SP, 0, 1)
    step_rows = min(key_span, all_keys.shape[0])
    needed = query_last // step_rows + 1

    def stats_turn(step_index, row_stats):
        offset = step_index * step_rows
        key_rows = lax.dynamic_slice_in_dim(all_keys, offset, step_rows, 0)
        return add_stats(row_stats, key_rows, offset)

    row_stats = lax.fori_loop(0, needed, stats_turn, start_stats)

    def values_turn(step_index, accumulated):
        offset = step_index * step_rows
        key_rows = lax.dynamic_slice_in_dim(all_keys, offset, step_rows, 0)
        value_rows = lax.dynamic_slice_in_dim(all_values, offset, step_rows, 0)
        return add_values(accumulated, key_rows, value_rows, offset, row_stats)

    attended = lax.fori_loop(0, needed, values_turn, start_values)
    attn_part = rms_scale(attended, head_gain).astype(jnp.bfloat16).reshape(length, width_c)
    summed = sum_at_owner(
        (
            jnp.dot(linear_part, out_linear, preferred_element_type=jnp.float32)
            + jnp.dot(attn_part, out_attn, preferred_element_type=jnp.float32)
        ).astype(jnp.bfloat16),
        "tp",
        0,
    )
    return summed.astype(jnp.bfloat16)


def solution(mesh):
    torus = Mesh(mesh.devices.reshape(16, 4, mesh.shape["tp"]), ("sp_0", "sp_1", "tp"))
    return jax.shard_map(
        shards,
        mesh=torus,
        in_specs=(
            P(SP_TP, None),
            P(),
            P(None, "tp"),
            P(None, "tp"),
            P(None, "tp"),
            P(),
            P(),
            P(None, "tp"),
            P(None, "tp"),
            P("tp"),
            P("tp"),
            P(SP, "tp"),
            P("tp"),
            P(None, "tp"),
            P(None, "tp"),
            P(None, "tp"),
            P(),
            P(),
            P("tp"),
            P(),
            P("tp", None),
            P("tp", None),
        ),
        out_specs=P(SP_TP, None),
        check_vma=False,
    )
```

profile of v0, /device:TPU:480, one launch (start us, length us, event | category | flops | bytes accessed | tf_op | source)
XLA Modules:
  0.0 508.7 jit_solution(14030344985649306292)
XLA Ops:
  6.5 1.1 fusion.67
  7.7 1.0 fusion.69
  8.7 1.1 broadcast_in_dim.88
  9.8 4.3 all-to-all-start
  14.1 1.2 copy.79
  15.9 6.5 %concatenate.76 = bf16[2048,896]{1,0:T(8,128)(2,1)} concatenate(bf16[2048,128]{1,0:T(8,128)(2,1)} %param.30, bf16[2048,128]{1,0:T(8,128)(2,1)} %param.31, bf16[2048,128]{1,0:T(8,128)(2,1)} %param.32, bf16[2048,64]{1,0:T(8,128)(2,1)S(1)} %copy.79, bf16[2048,64]{1,0:T(8,128)(2,1)S(1)} %copy.80, bf16[2048,128]{1,0:T(8,128)(2,1)} %param.41, bf16[2048,128]{1,0:T(8,128)(2,1)} %param.42, ...), dimensions={1} | concatenate | bytes 7340032 | tf_op jit(solution)/shard_map/concatenate | solution.py:171
  22.3 7.7 %all-to-all-done = bf16[8,32,2048]{2,1,0:T(8,128)(2,1)S(1)} async-done(((bf16[8,32,2048]{2,1,0:T(8,128)(2,1)}), bf16[8,32,2048]{2,1,0:T(8,128)(2,1)S(1)}, u32[]{:S(2)}, u32[]{:S(2)}) %all-to-all-start) | async-done | bytes 1048608 | tf_op jit(solution)/shard_map/all_to_all | solution.py:21
  30.0 3.3 convolution_convert_fusion
  36.4 96.7 %while.36 = (s32[]{:T(128)}, f32[2,64,128]{2,1,0:T(8,128)S(1)}, f32[4,2,64,128]{3,2,0,1:T(8,128)S(1)}, f32[4,2,64,64]{3,2,1,0:T(8,128)S(1)}, f32[4,2,64,64]{3,2,...) while((s32[]{:T(128)}, f32[2,64,128]{2,1,0:T(8,128)S(1)}, ...), condition=%wide.region_3.4_spmd, body=%wide.region_2.3_spmd.sunk | while | flops 36917248 | bytes 20173448 | solution.py:227
  36.6 4.2 fusion.306
  40.8 5.6 %copy.185 = f32[2,64,64,64]{1,2,3,0:T(8,128)} copy(f32[2,64,64,64]{3,2,1,0:T(8,128)} %get-tuple-element.512) | data formatting | bytes 4194304 | tf_op jit(solution)/shard_map/while
  46.4 5.6 %copy.189 = f32[2,64,64,64]{1,2,3,0:T(8,128)} copy(f32[2,64,64,64]{3,2,1,0:T(8,128)} %get-tuple-element.515) | data formatting | bytes 4194304 | tf_op jit(solution)/shard_map/while
  52.4 5.2 %fusion.307 = (f32[2,64,64]{1,2,0:T(8,128)S(1)}, bf16[2,64,64]{1,2,0:T(8,128)(2,1)S(1)}, bf16[2,64,64]{1,2,0:T(8,128)(2,1)S(1)}, bf16[2,64,64]{1,2,0:T(8,128)(2,1)S(1)}) fusion(f32[2,64,64,64]{1,2,3,0:T(8,128)} %copy.185, f32[2,64,64]{2,1,0:T(8,128)S(1)} %copy.186, f32[2,64,64]{2,1,0:T(8,128)S(1)} %copy.187, f32[2,64,64]{2,1,0:T(8,128)S(1)} %copy.188, ...), kind=kLoop, calls=%fused_computation.44.clone.1 | loop fusion | flops 6258688 | bytes 4407296 | tf_op jit(solution)/shard_map/while/body/eval_jaxpr/hin,hjn,hijn->hij/dot_general | solution.py:82
  60.7 4.2 fusion.306
  65.0 5.6 %copy.185 = f32[2,64,64,64]{1,2,3,0:T(8,128)} copy(f32[2,64,64,64]{3,2,1,0:T(8,128)} %get-tuple-element.512) | data formatting | bytes 4194304 | tf_op jit(solution)/shard_map/while
  70.6 5.6 %copy.189 = f32[2,64,64,64]{1,2,3,0:T(8,128)} copy(f32[2,64,64,64]{3,2,1,0:T(8,128)} %get-tuple-element.515) | data formatting | bytes 4194304 | tf_op jit(solution)/shard_map/while
  76.5 5.2 %fusion.307 = (f32[2,64,64]{1,2,0:T(8,128)S(1)}, bf16[2,64,64]{1,2,0:T(8,128)(2,1)S(1)}, bf16[2,64,64]{1,2,0:T(8,128)(2,1)S(1)}, bf16[2,64,64]{1,2,0:T(8,128)(2,1)S(1)}) fusion(f32[2,64,64,64]{1,2,3,0:T(8,128)} %copy.185, f32[2,64,64]{2,1,0:T(8,128)S(1)} %copy.186, f32[2,64,64]{2,1,0:T(8,128)S(1)} %copy.187, f32[2,64,64]{2,1,0:T(8,128)S(1)} %copy.188, ...), kind=kLoop, calls=%fused_computation.44.clone.1 | loop fusion | flops 6258688 | bytes 4407296 | tf_op jit(solution)/shard_map/while/body/eval_jaxpr/hin,hjn,hijn->hij/dot_general | solution.py:82
  84.9 4.2 fusion.306
  89.1 5.6 %copy.185 = f32[2,64,64,64]{1,2,3,0:T(8,128)} copy(f32[2,64,64,64]{3,2,1,0:T(8,128)} %get-tuple-element.512) | data formatting | bytes 4194304 | tf_op jit(solution)/shard_map/while
  94.7 5.6 %copy.189 = f32[2,64,64,64]{1,2,3,0:T(8,128)} copy(f32[2,64,64,64]{3,2,1,0:T(8,128)} %get-tuple-element.515) | data formatting | bytes 4194304 | tf_op jit(solution)/shard_map/while
  100.7 5.2 %fusion.307 = (f32[2,64,64]{1,2,0:T(8,128)S(1)}, bf16[2,64,64]{1,2,0:T(8,128)(2,1)S(1)}, bf16[2,64,64]{1,2,0:T(8,128)(2,1)S(1)}, bf16[2,64,64]{1,2,0:T(8,128)(2,1)S(1)}) fusion(f32[2,64,64,64]{1,2,3,0:T(8,128)} %copy.185, f32[2,64,64]{2,1,0:T(8,128)S(1)} %copy.186, f32[2,64,64]{2,1,0:T(8,128)S(1)} %copy.187, f32[2,64,64]{2,1,0:T(8,128)S(1)} %copy.188, ...), kind=kLoop, calls=%fused_computation.44.clone.1 | loop fusion | flops 6258688 | bytes 4407296 | tf_op jit(solution)/shard_map/while/body/eval_jaxpr/hin,hjn,hijn->hij/dot_general | solution.py:82
  109.1 4.2 fusion.306
  113.3 5.6 %copy.185 = f32[2,64,64,64]{1,2,3,0:T(8,128)} copy(f32[2,64,64,64]{3,2,1,0:T(8,128)} %get-tuple-element.512) | data formatting | bytes 4194304 | tf_op jit(solution)/shard_map/while
  118.9 5.6 %copy.189 = f32[2,64,64,64]{1,2,3,0:T(8,128)} copy(f32[2,64,64,64]{3,2,1,0:T(8,128)} %get-tuple-element.515) | data formatting | bytes 4194304 | tf_op jit(solution)/shard_map/while
  124.9 5.2 %fusion.307 = (f32[2,64,64]{1,2,0:T(8,128)S(1)}, bf16[2,64,64]{1,2,0:T(8,128)(2,1)S(1)}, bf16[2,64,64]{1,2,0:T(8,128)(2,1)S(1)}, bf16[2,64,64]{1,2,0:T(8,128)(2,1)S(1)}) fusion(f32[2,64,64,64]{1,2,3,0:T(8,128)} %copy.185, f32[2,64,64]{2,1,0:T(8,128)S(1)} %copy.186, f32[2,64,64]{2,1,0:T(8,128)S(1)} %copy.187, f32[2,64,64]{2,1,0:T(8,128)S(1)} %copy.188, ...), kind=kLoop, calls=%fused_computation.44.clone.1 | loop fusion | flops 6258688 | bytes 4407296 | tf_op jit(solution)/shard_map/while/body/eval_jaxpr/hin,hjn,hijn->hij/dot_general | solution.py:82
  133.1 12.8 %all-gather = f32[8,64,128]{2,1,0:T(8,128)S(1)} all-gather(f32[2,64,128]{2,1,0:T(8,128)S(1)} %get-tuple-element.146), channel_id=2, replica_groups=mesh['sp_0'=16,'sp_1'=4,'tp'=8] {'sp_1'}, dimensions={0}, use_global_device_ids=true | all-gather | bytes 327680 | tf_op jit(solution)/shard_map/all_gather | solution.py:44
  148.8 64.8 %all-gather.7.cloned.1.call-done = f32[32,64,128]{2,1,0:T(8,128)} async-done(((f32[2,64,128]{2,1,0:T(8,128)}), f32[32,64,128]{2,1,0:T(8,128)}) %all-gather.7.cloned.1.call-update) | async-done | bytes 1048592 | tf_op jit(solution)/shard_map/all_gather | solution.py:44
  213.6 1.6 fusion.154
  229.8 1.1 fusion.66
  231.8 137.7 %all-gather.5.cloned.1.call-done = bf16[16384,256]{1,0:T(8,128)(2,1)} async-done(((bf16[256,256]{1,0:T(8,128)(2,1)}), bf16[16384,256]{1,0:T(8,128)(2,1)}) %all-gather.5.cloned.1.call-update) | async-done | bytes 8388624 | tf_op jit(solution)/shard_map/all_gather | solution.py:57
  369.5 5.7 %fusion.153 = (bf16[16384,128]{1,0:T(8,128)(2,1)}, bf16[16384,128]{1,0:T(8,128)(2,1)}) fusion(bf16[16384,256]{1,0:T(8,128)(2,1)} %all-gather.5.cloned.1.call-done), kind=kLoop, calls=%fused_computation.253 | loop fusion | bytes 16777216 | tf_op jit(solution)/shard_map/split | solution.py:58
  375.2 6.4 %copy.99 = bf16[16384,128]{0,1:T(8,128)(2,1)} copy(bf16[16384,128]{1,0:T(8,128)(2,1)} %get-tuple-element.313) | data formatting | bytes 8388608
  381.6 36.9 %while.37 = (s32[]{:T(128)}, f32[1,2,256]{2,1,0:T(2,128)S(1)}, f32[1,2,256]{2,1,0:T(2,128)S(1)}, s32[]{:T(128)}, bf16[16384,128]{0,1:T(8,128)(2,1)}, /*index=5*/...) while((s32[]{:T(128)}, f32[1,2,256]{2,1,0:T(2,128)S(1)}, ...), condition=%wide.region_11.12_spmd.clone, body=%wide.region_8.11_spmd.clone.sunk | while | flops 71043336 | bytes 5869735 | solution.py:306
  383.9 1.0 constant_dynamic-slice_fusion.4
  386.2 1.0 constant_dynamic-slice_fusion.4
  388.5 1.0 constant_dynamic-slice_fusion.4
  390.8 1.0 constant_dynamic-slice_fusion.4
  393.2 1.0 constant_dynamic-slice_fusion.4
  395.5 1.0 constant_dynamic-slice_fusion.4
  397.8 1.0 constant_dynamic-slice_fusion.4
  400.1 1.0 constant_dynamic-slice_fusion.4
  402.4 1.0 constant_dynamic-slice_fusion.4
  404.7 1.0 constant_dynamic-slice_fusion.4
  407.0 1.0 constant_dynamic-slice_fusion.4
  409.3 1.0 constant_dynamic-slice_fusion.4
  418.6 62.0 %while.38 = (s32[]{:T(128)}, f32[256,1,128]{0,2,1:T(8,128)S(1)}, s32[]{:T(128)}, bf16[16384,128]{1,0:T(8,128)(2,1)}, bf16[16384,128]{0,1:T(8,128)(2,1)}, /*index...) while((s32[]{:T(128)}, f32[256,1,128]{0,2,1:T(8,128)S(1)}, ...), condition=%wide.region_13.14_spmd.clone, body=%wide.region_12.13_spmd.clone.sunk | while | flops 137397504 | bytes 6109891 | solution.py:314
  418.6 1.0 constant_dynamic-slice_fusion.5
  420.6 1.9 fusion.324
  424.5 1.9 fusion.324
  428.4 1.9 fusion.324
  432.2 1.9 fusion.324
  436.1 1.9 fusion.324
  440.0 1.9 fusion.324
  443.9 1.9 fusion.324
  447.7 1.9 fusion.324
  451.6 1.9 fusion.324
  455.5 1.9 fusion.324
  459.3 1.9 fusion.324
  463.2 1.9 fusion.324
  467.1 1.9 fusion.324
  470.9 1.9 fusion.324
  474.8 1.9 fusion.324
  478.7 1.9 fusion.324
  481.2 19.9 %all_to_all.10 = bf16[8,32,2048]{2,1,0:T(8,128)(2,1)S(1)} all-to-all(bf16[8,32,2048]{2,1,0:T(8,128)(2,1)S(1)} %bitcast.325), channel_id=1, replica_groups=mesh['sp_0'=16,'sp_1'=4,'tp'=8] {'tp'}, dimensions={0} | all-to-all | bytes 2097152 | tf_op jit(solution)/shard_map/all_to_all | solution.py:69
  (441 shorter events, 90.4 us)
Async XLA Ops:
  6.5 224.8 %copy-start = (bf16[128,2048]{1,0:T(8,128)(2,1)S(1)}, bf16[128,2048]{1,0:T(8,128)(2,1)}, u32[]{:S(2)}) copy-start(bf16[128,2048]{1,0:T(8,128)(2,1)} %param.48) | copy-start | bytes 1572868
  6.5 8.8 %copy-start.4 = (bf16[2048,64]{0,1:T(8,128)(2,1)S(1)}, bf16[2048,64]{0,1:T(8,128)(2,1)}, u32[]{:S(2)}) copy-start(bf16[2048,64]{0,1:T(8,128)(2,1)} %param.34) | copy-start | bytes 786436
  6.5 9.1 %copy-start.12 = (f32[64]{0:T(128)S(1)}, f32[64]{0:T(128)}, u32[]{:S(2)}) copy-start(f32[64]{0:T(128)} %param.45) | copy-start | bytes 772
  6.5 9.2 %copy-start.7 = (f32[256,2]{0,1:T(2,128)S(1)}, f32[256,2]{0,1:T(2,128)}, u32[]{:S(2)}) copy-start(f32[256,2]{0,1:T(2,128)} %param.39) | copy-start | bytes 6148
  9.8 20.2 %all-to-all-start = ((bf16[8,32,2048]{2,1,0:T(8,128)(2,1)}), bf16[8,32,2048]{2,1,0:T(8,128)(2,1)S(1)}, u32[]{:S(2)}, u32[]{:S(2)}) async-start(bf16[8,32,2048]{2,1,0:T(8,128)(2,1)} %broadcast_in_dim.88), calls=%async_computation | async-start | bytes 2097152 | tf_op jit(solution)/shard_map/all_to_all | solution.py:21
  14.1 199.5 %all-gather.7.cloned.1.call-start = ((), (), s32[]{:S(2)}) async-start(), calls=%async_computation.3 | async-start | bytes 1114112 | tf_op jit(solution)/shard_map/all_gather | solution.py:44
  30.0 4.8 copy-start.11
  30.0 4.8 copy-start.13
  30.0 5.5 %copy-start.6 = (bf16[64,128]{1,0:T(8,128)(2,1)S(1)}, bf16[64,128]{1,0:T(8,128)(2,1)}, u32[]{:S(2)}) copy-start(bf16[64,128]{1,0:T(8,128)(2,1)} %param.35) | copy-start | bytes 49156
  30.0 5.5 %copy-start.8 = (f32[128]{0:T(128)S(1)}, f32[128]{0:T(128)}, u32[]{:S(2)}) copy-start(f32[128]{0:T(128)} %param.37) | copy-start | bytes 1540
  33.4 3.0 copy-start.1
  36.3 110.9 %copy-start.5 = (bf16[256,128]{1,0:T(8,128)(2,1)S(1)}, bf16[256,128]{1,0:T(8,128)(2,1)}, u32[]{:S(2)}) copy-start(bf16[256,128]{1,0:T(8,128)(2,1)} %get-tuple-element.334) | copy-start | bytes 196612
  36.4 111.6 %copy-start.14 = (f32[128]{0:T(128)S(1)}, f32[128]{0:T(128)}, u32[]{:S(2)}) copy-start(f32[128]{0:T(128)} %param.40) | copy-start | bytes 1540
  36.4 111.7 %copy-start.2 = (f32[256,128]{1,0:T(8,128)S(1)}, f32[256,128]{1,0:T(8,128)}, u32[]{:S(2)}) copy-start(f32[256,128]{1,0:T(8,128)} %get-tuple-element.333) | copy-start | bytes 393220
  36.4 112.3 %copy-start.9 = (f32[64]{0:T(128)S(1)}, f32[64]{0:T(128)}, u32[]{:S(2)}) copy-start(f32[64]{0:T(128)} %param.44) | copy-start | bytes 772
  147.2 222.3 %all-gather.5.cloned.1.call-start = ((), (), s32[]{:S(2)}) async-start(), calls=%async_computation.2 | async-start | bytes 8519680 | tf_op jit(solution)/shard_map/all_gather | solution.py:57
  418.6 62.1 %copy-start.3 = (bf16[128,2048]{1,0:T(8,128)(2,1)S(1)}, bf16[128,2048]{1,0:T(8,128)(2,1)}, u32[]{:S(2)}) copy-start(bf16[128,2048]{1,0:T(8,128)(2,1)} %param.49) | copy-start | bytes 1572868
  418.6 62.1 %copy-start.10 = (f32[128]{0:T(128)S(1)}, f32[128]{0:T(128)}, u32[]{:S(2)}) copy-start(f32[128]{0:T(128)} %param.47) | copy-start | bytes 1540
Sparse Core Ops, SparseCore 0:
  147.3 66.2 all-gather.6
  216.5 152.9 all-gather.4
where the time goes:
time: 512 us; the launch traced here: 509 us
  waiting for transfers between devices  210 us (41%)
  local copies, waits for them, and re-layouts  103 us (20%)
  matrix products  84.1 us (16%)
  other arithmetic  57.8 us (11%)
  blocking collectives  32.7 us (6%)
  between operations  14.2 us (3%)
    all_gather x1, waiting for transfers between devices, side_by_side(): whole = lax.all_gather(both, axis, axis=dim, tiled=True)  138 us
    all_gather x1, waiting for transfers between devices, prefix_by_axis(): pieces = lax.all_gather(subtotal, axis)  64.8 us
    while x24, local copies, waits for them, and re-layouts  44.9 us
    dot_general x16, matrix products, add_values(): jnp.einsum('hqk,khe->qhe', weights, value_heads, preferred_element_type=j...  30.2 us
    dot_general x4, other arithmetic, ratio_dots(): return jnp.einsum('hin,hjn,hijn->hij', left, right, ratios)  20.7 us
    dot_general x32, matrix products, block_scores(): jnp.einsum('qhmd,khmd->hmqk', queries, key_heads, preferred_element_type=...  20.1 us
    all_to_all x1, blocking collectives, sum_at_owner(): lax.all_to_all(blocks, axis, split_axis=0, concat_axis=0, tiled=True)  19.9 us
    exp x4, other arithmetic, block_step(): jnp.exp(jnp.where(lower_incl[None, :, :, None], spread, -jnp.inf))  16.9 us
  transfers between devices with their start and end apart: 3, of which 3 were waited for; matrix products, arithmetic and copies ran while one was open for 5% of the time, Pallas kernels for 0%

commit v1 on v0

v1 whole, which is shorter than its diff:
```python
import functools

import jax
import jax.numpy as jnp
from jax import lax
from jax.experimental import pallas as pl
from jax.experimental.pallas import tpu as pltpu
from jax.sharding import Mesh
from jax.sharding import PartitionSpec as P

HALF = 64
LANES = 128
F32 = jnp.float32
BF16 = jnp.bfloat16
NORM_EPS = 1e-06
GROUP_EPS = 0.00064
LOG2E = 1.4426950408889634
SCORE = HALF ** (-0.5) * LOG2E
FLOOR = -1e29
MASKED = -1e30
STATS = 16
VMEM_LIMIT = 56 * 1024 * 1024


def vmem():
    return pl.BlockSpec(memory_space=pltpu.VMEM)


def smem():
    return pl.BlockSpec(memory_space=pltpu.SMEM)


def params():
    return pltpu.CompilerParams(vmem_limit_bytes=VMEM_LIMIT)


def cost(flops, size):
    return pl.CostEstimate(flops=flops, bytes_accessed=size, transcendentals=0)


def low_lanes(shape=(1, LANES)):
    return lax.broadcasted_iota(jnp.int32, shape, len(shape) - 1) < HALF


def half_sums(v):
    low = low_lanes()
    first = jnp.sum(jnp.where(low, v, 0.0), -1, keepdims=True)
    second = jnp.sum(jnp.where(low, 0.0, v), -1, keepdims=True)
    return jnp.where(low, first, second)


def dot(a, b):
    return jnp.dot(a, b, preferred_element_type=F32)


def dot_nt(a, b):
    return lax.dot_general(a, b, (((1,), (1,)), ((), ())), preferred_element_type=F32)


def dot_tn(a, b):
    return lax.dot_general(a, b, (((0,), (0,)), ((), ())), preferred_element_type=F32)


def two_parts(v):
    high = v.astype(BF16)
    return high, (v - high.astype(F32)).astype(BF16)


def dot3(a, b):
    ah, al = two_parts(a)
    bh, bl = two_parts(b)
    return dot(ah, bh) + (dot(ah, bl) + dot(al, bh))


def rounded(v):
    return v.astype(BF16).astype(F32)


def qkv_kernel(x_ref, gain_ref, wq_ref, wk_ref, wv_ref, qg_ref, kg_ref, normed_ref, q_ref, kv_ref):
    rows = x_ref.shape[0]
    step = 32

    def turn(i, carry):
        span = pl.ds(pl.multiple_of(i * step, step), step)
        x = x_ref[span, :].astype(F32)
        scale = lax.rsqrt(jnp.mean(x * x, -1, keepdims=True) + NORM_EPS)
        normed_ref[span, :] = (x * scale * gain_ref[...]).astype(BF16)
        return carry

    lax.fori_loop(0, rows // step, turn, 0)
    normed = normed_ref[...]

    def map_norm(weight_ref, gain_ref):
        v = rounded(dot(normed, weight_ref[...]))
        scale = lax.rsqrt(half_sums(v * v) * (1.0 / HALF) + NORM_EPS)
        return (v * scale * gain_ref[...]).astype(BF16)

    q_ref[...] = map_norm(wq_ref, qg_ref)
    kv_ref[:, :LANES] = map_norm(wk_ref, kg_ref)
    kv_ref[:, LANES:] = dot(normed, wv_ref[...]).astype(BF16)


def linear_kernel(
    normed_ref,
    wr_ref,
    wk_ref,
    wv_ref,
    wd_ref,
    wg_ref,
    du_ref,
    ru_ref,
    db_ref,
    rb_ref,
    extra_ref,
    extra_t_ref,
    qh_ref,
    ol_ref,
    map_ref,
):
    normed = normed_ref[...]
    length = normed.shape[0]
    low = low_lanes()
    recept = rounded(dot(normed, wr_ref[...]))
    key = rounded(dot(normed, wk_ref[...]))
    value = rounded(dot(normed, wv_ref[...]))
    decay_low = dot(normed, wd_ref[...]).astype(BF16)
    rate_low = dot(normed, wg_ref[...]).astype(BF16)
    log_chan = -jnp.exp(db_ref[...] + jnp.tanh(dot(decay_low, du_ref[...])))
    gate = jax.nn.sigmoid(rb_ref[...] + jnp.tanh(dot(rate_low, ru_ref[...])))
    unit = key * lax.rsqrt(half_sums(key * key) + NORM_EPS)
    extra = extra_ref[...]
    head_step = jnp.where(low, extra[:, 0:1], extra[:, 1:2])
    row = lax.broadcasted_iota(jnp.int32, (length, length), 0)
    col = lax.broadcasted_iota(jnp.int32, (length, length), 1)
    incl = row >= col
    lower = jnp.where(incl, 1.0, 0.0).astype(F32)
    both = jnp.dot(
        lower,
        jnp.concatenate([log_chan, head_step], axis=1),
        preferred_element_type=F32,
        precision=lax.Precision.HIGHEST,
    )
    chan = both[:, :LANES]
    head = both[:, LANES:]
    head_rows = jnp.dot(
        extra_t_ref[...],
        jnp.where(row <= col, 1.0, 0.0).astype(F32),
        preferred_element_type=F32,
        precision=lax.Precision.HIGHEST,
    )
    chan_prev = chan - log_chan
    head_prev = head - head_step
    remove = -unit
    restore = unit * gate
    inject = key * gate
    total = chan + head
    ending = total[length - 1 : length, :]
    to_end = jnp.exp(jnp.minimum(ending - total, 0.0))
    grow = jnp.exp(chan)
    shrink = jnp.exp(-chan)
    left = jnp.concatenate([remove * jnp.exp(chan_prev), recept * grow], axis=0)
    right = jnp.concatenate([restore * shrink, inject * shrink], axis=0).astype(BF16)
    remove_dec = remove * jnp.exp(chan_prev + head_prev)
    recept_dec = recept * jnp.exp(total)
    restore_end = restore * to_end
    inject_end = inject * to_end
    turned = pltpu.roll(value, HALF, 1)
    outs = []
    maps = []
    for h in range(2):
        own = low if h == 0 else jnp.logical_not(low)
        products = dot_nt(jnp.where(own, left, 0.0).astype(BF16), right)
        spread = head[:, h * HALF : h * HALF + 1] - head_rows[h : h + 1, :]
        ratio_incl = jnp.exp(jnp.where(incl, spread, MASKED))
        ratio_strict = jnp.exp(
            jnp.where(row > col, spread - head_step[:, h * HALF : h * HALF + 1], MASKED)
        )
        low_restore = products[:length, :length] * ratio_strict
        low_inject = (products[:length, length:] * ratio_strict).astype(BF16)
        out_restore = (products[length:, :length] * ratio_incl).astype(BF16)
        out_inject = (products[length:, length:] * ratio_incl).astype(BF16)
        inverse = jnp.where(row == col, 1.0, 0.0).astype(F32)
        for level in range((length - 1).bit_length()):
            joint = jnp.right_shift(row, level + 1) == jnp.right_shift(col, level + 1)
            block = joint & (jnp.right_shift(row, level) > jnp.right_shift(col, level))
            part = jnp.where(block, low_restore, 0.0)
            if level == 0:
                inverse = inverse + part
            else:
                known = inverse.astype(BF16)
                inverse = inverse + dot(known, dot(part.astype(BF16), known).astype(BF16))
        other = jnp.where(own, 0.0, turned).astype(BF16)
        sides = jnp.where(own, remove_dec, dot(low_inject, other)).astype(BF16)
        along = dot(inverse.astype(BF16), sides).astype(BF16)
        outs.append(
            dot(out_restore, along) + jnp.where(own, recept_dec, dot(out_inject, other))
        )
        maps.append(
            dot_tn(jnp.where(own, restore_end, 0.0).astype(BF16), along)
            + dot_tn(jnp.where(own, inject_end, 0.0).astype(BF16), other)
        )
    qh_ref[...] = jnp.where(low, outs[0], outs[1]).astype(BF16)
    ol_ref[...] = jnp.where(low, outs[1], outs[0])
    r128 = lax.broadcasted_iota(jnp.int32, (LANES, LANES), 0)
    c128 = lax.broadcasted_iota(jnp.int32, (LANES, LANES), 1)
    map_ref[...] = (
        maps[0] + maps[1] + jnp.where(r128 == c128, jnp.exp(ending) - 1.0, 0.0)
    ).astype(BF16)


def map_masks():
    r = lax.broadcasted_iota(jnp.int32, (LANES, LANES), 0)
    c = lax.broadcasted_iota(jnp.int32, (LANES, LANES), 1)
    same = (r < HALF) == (c < HALF)
    return same, jnp.where(r == c, 1.0, 0.0).astype(F32)


def compose(later, earlier, same):
    return dot3(jnp.where(same, later, 0.0), earlier) + jnp.where(same, 0.0, later)


def row_kernel(place_ref, maps_ref, total_ref, before_ref):
    y = place_ref[1]
    same, eye = map_masks()
    peers, rows, _ = maps_ref.shape
    so_far = eye
    before = eye
    for k in range(peers):
        before = jnp.where(y == k, so_far, before)
        one = maps_ref[k, rows - LANES :, :].astype(F32) + eye
        so_far = one if k == 0 else compose(one, so_far, same)
    before_ref[...] = before
    total_ref[...] = (so_far - eye).astype(BF16)


def carry_kernel(place_ref, totals_ref, before_ref, state_ref):
    z = place_ref[0]
    same, eye = map_masks()
    peers = totals_ref.shape[0]
    level = [
        jnp.where(k < z, totals_ref[k].astype(F32), 0.0) + eye for k in range(peers)
    ]
    while len(level) > 1:
        level = [compose(level[k + 1], level[k], same) for k in range(0, len(level), 2)]
    full = compose(before_ref[...], level[0], same)
    state_ref[...] = jnp.where(same, 0.0, full).astype(BF16)


def attend_kernel(place_ref, q_ref, kv_ref, out_ref, top_ref, acc_ref, wide_ref):
    z = place_ref[0]
    y = place_ref[1]
    rows_q = q_ref.shape[0]
    blk = 256
    span = 1024
    low = low_lanes()
    wide_ref[:, :LANES] = kv_ref[:, LANES:]
    wide_ref[:, LANES:] = jnp.ones((kv_ref.shape[0], LANES), BF16)
    top_ref[...] = jnp.full(top_ref.shape, FLOOR, F32)
    acc_ref[...] = jnp.zeros(acc_ref.shape, F32)

    def step(start, masked):
        keys = kv_ref[pl.ds(start, span), :LANES]
        wide = wide_ref[pl.ds(start, span), :]
        for t in range(rows_q):
            q = q_ref[t, :blk, :]
            if masked:
                row = lax.broadcasted_iota(jnp.int32, (blk, span), 0) + (z * rows_q + t) * blk
                col = lax.broadcasted_iota(jnp.int32, (blk, span), 1)
                k_place = (jnp.right_shift(col, 8) + jnp.right_shift(start, 8)) * rows_q + y
                allowed = row >= k_place * blk + jnp.bitwise_and(col, blk - 1)
            for m in range(2):
                own = low if m == 0 else jnp.logical_not(low)
                s = dot_nt(jnp.where(own, q, jnp.zeros_like(q)), keys) * SCORE
                if masked:
                    s = jnp.where(allowed, s, MASKED)
                at = 2 * t + m
                old = top_ref[at, :, 0:1]
                new = jnp.maximum(old, jnp.max(s, -1, keepdims=True))
                p = jnp.exp2(s - new).astype(BF16)
                acc_ref[at] = acc_ref[at] * jnp.exp2(old - new) + dot(p, wide)
                top_ref[at] = jnp.broadcast_to(new, (blk, LANES))

    whole = (z * blk) // span

    def turn(i, carry):
        step(pl.multiple_of(i * span, span), False)
        return carry

    lax.fori_loop(0, whole, turn, 0)
    step(pl.multiple_of(whole * span, span), True)
    lane = lax.broadcasted_iota(jnp.int32, (1, LANES), 1)
    for t in range(rows_q):
        stats = jnp.zeros((blk, LANES), F32)
        for m in range(2):
            at = 2 * t + m
            acc = acc_ref[at]
            weight = acc[:, LANES : LANES + 1]
            seen = weight > 0.0
            safe = jnp.where(seen, weight, 1.0)
            out_ref[t, :blk, m * LANES : (m + 1) * LANES] = (acc[:, :LANES] / safe).astype(BF16)
            lse = jnp.where(seen, top_ref[at, :, 0:1] + jnp.log2(safe), MASKED)
            high = rounded(lse)
            mid = rounded(lse - high)
            tail = rounded(lse - high - mid)
            stats = jnp.where(lane == m, high, stats)
            stats = jnp.where(lane == 2 + m, mid, stats)
            stats = jnp.where(lane == 4 + m, tail, stats)
        out_ref[t, blk:, :] = stats.T[:STATS, :].astype(BF16)


def finish_kernel(
    lam_ref, parts_ref, hg_ref, qh_ref, ol_ref, state_ref, gg_ref, wl_ref, wa_ref, out_ref
):
    blk = qh_ref.shape[0]
    peers = parts_ref.shape[0]
    lam = lam_ref[0]
    stats = jnp.concatenate(
        [parts_ref[j, blk:, :].astype(F32) for j in range(peers)]
        + [jnp.zeros((LANES - peers * STATS, blk), F32)],
        axis=0,
    ).T
    attended = jnp.zeros((blk, LANES), F32)
    for m in range(2):
        lses = []
        for j in range(peers):
            at = j * STATS + m
            lses.append(
                stats[:, at : at + 1] + stats[:, at + 2 : at + 3] + stats[:, at + 4 : at + 5]
            )
        top = functools.reduce(jnp.maximum, lses)
        shares = [jnp.exp2(v - top) for v in lses]
        whole = functools.reduce(jnp.add, shares)
        mixed = jnp.zeros((blk, LANES), F32)
        for j in range(peers):
            part = parts_ref[j, :blk, m * LANES : (m + 1) * LANES].astype(F32)
            mixed = mixed + part * (shares[j] / whole)
        attended = mixed if m == 0 else attended - lam * mixed
    scale = lax.rsqrt(jnp.mean(attended * attended, -1, keepdims=True) + NORM_EPS)
    attn = (attended * scale * hg_ref[...]).astype(BF16)
    read = dot(qh_ref[...], state_ref[...]) + ol_ref[...]
    centered = read - half_sums(read) * (1.0 / HALF)
    var = half_sums(centered * centered) * (1.0 / HALF)
    linear = centered * lax.rsqrt(var + GROUP_EPS)
    linear = (pltpu.roll(linear, HALF, 1) * gg_ref[...]).astype(BF16)
    width = 512
    for c in range(0, out_ref.shape[1], width):
        out_ref[:, c : c + width] = (
            dot(linear, wl_ref[:, c : c + width]) + dot(attn, wa_ref[:, c : c + width])
        ).astype(BF16)


def copy_for_each(x, axis):
    copies = jnp.broadcast_to(x, (lax.axis_size(axis), *x.shape))
    return lax.all_to_all(copies, axis, split_axis=0, concat_axis=0, tiled=True)


def shards(
    tokens,
    norm_gain,
    recept_weight,
    key_weight,
    value_weight,
    decay_down_weight,
    rate_down,
    decay_up,
    rate_up,
    decay_base,
    rate_base,
    decay_extra,
    group_gain,
    attn_query,
    attn_key,
    attn_value,
    query_gain,
    key_gain,
    lambdas,
    head_gain,
    out_linear,
    out_attn,
):
    shape = jax.ShapeDtypeStruct
    depth = tokens.shape[1]
    peers = lax.axis_size("tp")
    length = tokens.shape[0] * peers
    place = jnp.stack([lax.axis_index("z"), lax.axis_index("y")]).astype(jnp.int32)
    line = lambda v: v.reshape(1, -1)
    rows = copy_for_each(tokens, "tp").reshape(length, depth)
    normed, query, key_value = pl.pallas_call(
        qkv_kernel,
        out_shape=(
            shape((length, depth), BF16),
            shape((length, LANES), BF16),
            shape((length, 2 * LANES), BF16),
        ),
        in_specs=[vmem()] * 7,
        out_specs=(vmem(),) * 3,
        compiler_params=params(),
        cost_estimate=cost(2 * length * depth * 384, 6 << 20),
        name="qkv",
    )(
        rows,
        line(norm_gain),
        attn_query,
        attn_key,
        attn_value,
        line(jnp.tile(query_gain, 2)),
        line(jnp.tile(key_gain, 2)),
    )
    all_kv = lax.all_gather(key_value, "z", axis=0, tiled=True)
    reader, local_out, state_map = pl.pallas_call(
        linear_kernel,
        out_shape=(
            shape((length, LANES), BF16),
            shape((length, LANES), F32),
            shape((LANES, LANES), BF16),
        ),
        in_specs=[vmem()] * 12,
        out_specs=(vmem(),) * 3,
        compiler_params=params(),
        cost_estimate=cost(2 * length * depth * 1024, 6 << 20),
        name="linear",
    )(
        normed,
        recept_weight,
        key_weight,
        value_weight,
        decay_down_weight,
        rate_down,
        decay_up,
        rate_up,
        line(decay_base),
        line(rate_base),
        decay_extra,
        decay_extra.T,
    )
    gathered = lax.all_gather(jnp.concatenate([query, state_map], axis=0), "y")
    total, before = pl.pallas_call(
        row_kernel,
        out_shape=(shape((LANES, LANES), BF16), shape((LANES, LANES), F32)),
        in_specs=[smem(), vmem()],
        out_specs=(vmem(),) * 2,
        compiler_params=params(),
        cost_estimate=cost(1 << 27, 1 << 20),
        name="row",
    )(place, gathered)
    totals = lax.all_gather(total, "z")
    state = pl.pallas_call(
        carry_kernel,
        out_shape=shape((LANES, LANES), BF16),
        in_specs=[smem(), vmem(), vmem()],
        out_specs=vmem(),
        compiler_params=params(),
        cost_estimate=cost(1 << 27, 1 << 20),
        name="carry",
    )(place, totals, before)
    all_kv, state = lax.optimization_barrier((all_kv, state))
    rows_q = gathered.shape[0]
    partial = pl.pallas_call(
        attend_kernel,
        out_shape=shape((rows_q, length + STATS, 2 * LANES), BF16),
        in_specs=[smem(), vmem(), vmem()],
        out_specs=vmem(),
        scratch_shapes=[
            pltpu.VMEM((2 * rows_q, length, LANES), F32),
            pltpu.VMEM((2 * rows_q, length, 2 * LANES), F32),
            pltpu.VMEM((all_kv.shape[0], 2 * LANES), BF16),
        ],
        compiler_params=params(),
        cost_estimate=cost(4 * rows_q * length * all_kv.shape[0] * 384, 6 << 20),
        name="attend",
    )(place, gathered, all_kv)
    parts = lax.all_to_all(partial, "y", split_axis=0, concat_axis=0, tiled=True)
    share = pl.pallas_call(
        finish_kernel,
        out_shape=shape((length, depth), BF16),
        in_specs=[smem()] + [vmem()] * 8,
        out_specs=vmem(),
        compiler_params=params(),
        cost_estimate=cost(2 * length * depth * 256, 4 << 20),
        name="finish",
    )(
        lambdas,
        parts,
        line(head_gain),
        reader,
        local_out,
        state,
        line(group_gain),
        out_linear,
        out_attn,
    )
    arrived = lax.all_to_all(
        share.reshape(peers, length // peers, depth), "tp", split_axis=0, concat_axis=0, tiled=True
    )
    return arrived.astype(F32).sum(axis=0).astype(BF16)


def solution(mesh):
    torus = Mesh(mesh.devices.reshape(16, 4, mesh.shape["tp"]), ("z", "y", "tp"))
    seq = ("z", "y")
    return jax.shard_map(
        shards,
        mesh=torus,
        in_specs=(
            P(("z", "y", "tp"), None),
            P(),
            P(None, "tp"),
            P(None, "tp"),
            P(None, "tp"),
            P(),
            P(),
            P(None, "tp"),
            P(None, "tp"),
            P("tp"),
            P("tp"),
            P(seq, "tp"),
            P("tp"),
            P(None, "tp"),
            P(None, "tp"),
            P(None, "tp"),
            P(),
            P(),
            P("tp"),
            P(),
            P("tp", None),
            P("tp", None),
        ),
        out_specs=P(("z", "y", "tp"), None),
        check_vma=False,
    )
```

time: 512 us -> 168 us (0.33)
  waiting for transfers between devices: 210 us -> 24.1 us
  local copies, waits for them, and re-layouts: 103 us -> 7.91 us
  matrix products: 84.1 us -> 0 us
  other arithmetic: 57.8 us -> 2.14 us
  Pallas kernels: 0 us -> 42.4 us
  blocking collectives: 32.7 us -> 68 us
    all_gather x2 -> x1, waiting for transfers between devices: 202 us -> 1.88 us  [shards(): all_kv = lax.all_gather(key_value, 'z', axis=0, tiled=True)]
    dot_general x147 -> x0, matrix products: 84.1 us -> none  [the longest x16 30.2 us: add_values(): jnp.einsum('hqk,khe->qhe', weights, value_heads, preferred_element_type=j...]
    while x24 -> x0, local copies, waits for them, and re-layouts: 44.9 us -> none
    pallas_call x0 -> x6, Pallas kernels: none -> 42.4 us  [the longest x1 17.2 us: shards(): pl.pallas_call(attend_kernel, out_shape=shape((rows_q, length + STATS, 2...]
    all_gather x1 -> x2, blocking collectives: 12.8 us -> 47.5 us  [the longest x1 33.7 us: shards(): totals = lax.all_gather(total, 'z')]
    dynamic_slice x32 -> x0, local copies, waits for them, and re-layouts: 31.2 us -> none  [the longest x16 15.6 us: values_turn(): key_rows = lax.dynamic_slice_in_dim(all_keys, offset, step_rows, 0)]
    dot_general x4 -> x0, other arithmetic: 20.7 us -> none  [ratio_dots(): return jnp.einsum('hin,hjn,hijn->hij', left, right, ratios)]
    exp x4 -> x0, other arithmetic: 16.9 us -> none  [block_step(): jnp.exp(jnp.where(lower_incl[None, :, :, None], spread, -jnp.inf))]
  transfers between devices with their start and end apart: 3 -> 3, of which waited for: 3 -> 3; matrix products, arithmetic and copies ran while one was open for 5% -> 3% of each run, Pallas kernels for 0% -> 10%
where the time goes in v1:
time: 168 us; the launch traced here: 167 us
  blocking collectives  68 us (40%)
  Pallas kernels  42.4 us (25%)
  waiting for transfers between devices  24.1 us (14%)
  between operations  14.1 us (8%)
  starting transfers between devices  8.58 us (5%)
  local copies, waits for them, and re-layouts  7.91 us (5%)
  other arithmetic  2.14 us (1%)
    all_gather x1, blocking collectives, shards(): totals = lax.all_gather(total, 'z')  33.7 us
    all_to_all x1, blocking collectives, shards(): lax.all_to_all(share.reshape(peers, length // peers, depth), 'tp', split_...  20.5 us
    pallas_call x1, Pallas kernels, shards(): pl.pallas_call(attend_kernel, out_shape=shape((rows_q, length + STATS, 2...  17.2 us
    all_to_all x1, waiting for transfers between devices, copy_for_each(): return lax.all_to_all(copies, axis, split_axis=0, concat_axis=0, tiled=True)  14.6 us
    all_gather x1, blocking collectives, shards(): gathered = lax.all_gather(jnp.concatenate([query, state_map], axis=0), 'y')  13.8 us
    pallas_call x1, Pallas kernels, shards(): pl.pallas_call(linear_kernel, out_shape=(shape((length, LANES), BF16), sh...  11.1 us
    all_to_all x1, waiting for transfers between devices, shards(): lax.all_to_all(partial, 'y', split_axis=0, concat_axis=0, tiled=True)  7.61 us
    pallas_call x1, Pallas kernels, shards(): pl.pallas_call(finish_kernel, out_shape=shape((length, depth), BF16), in_...  4.94 us
  transfers between devices with their start and end apart: 3, of which 3 were waited for; matrix products, arithmetic and copies ran while one was open for 3% of the time, Pallas kernels for 10%

profile of v1, /device:TPU:480, one launch (start us, length us, event | category | flops | bytes accessed | tf_op | source)
XLA Modules:
  0.0 167.3 jit_solution(11268500041102529226)
XLA Ops:
  6.5 0.0 copy-start.6
  6.5 0.0 copy-start.7
  6.5 2.0 %broadcast_in_dim.3 = bf16[8,32,2048]{2,1,0:T(8,128)(2,1)} broadcast(bf16[32,2048]{1,0:T(8,128)(2,1)} %param.22), dimensions={1,2} | broadcast | bytes 1179648 | tf_op jit(solution)/shard_map/broadcast_in_dim | solution.py:353
  8.6 0.0 copy-start.2
  8.6 4.4 %all-to-all-start = ((bf16[8,32,2048]{2,1,0:T(8,128)(2,1)}), bf16[8,32,2048]{2,1,0:T(8,128)(2,1)S(1)}, u32[]{:S(2)}, u32[]{:S(2)}) async-start(bf16[8,32,2048]{2,1,0:T(8,128)(2,1)} %broadcast_in_dim.3), calls=%async_computation | async-start | bytes 2097152 | tf_op jit(solution)/shard_map/all_to_all | solution.py:354
  13.0 0.0 copy-start.3
  13.0 0.0 all-gather.4.cloned.1.call-start
  13.1 0.0 copy-done.6
  13.1 0.6 reshape_tile.6.qg_ref
  13.7 0.0 copy-done.7
  13.7 0.6 reshape_tile.7.kg_ref
  14.3 14.6 %all-to-all-done = bf16[8,32,2048]{2,1,0:T(8,128)(2,1)S(1)} async-done(((bf16[8,32,2048]{2,1,0:T(8,128)(2,1)}), bf16[8,32,2048]{2,1,0:T(8,128)(2,1)S(1)}, u32[]{:S(2)}, u32[]{:S(2)}) %all-to-all-start) | async-done | bytes 1048608 | tf_op jit(solution)/shard_map/all_to_all | solution.py:354
  28.9 0.0 copy-start
  28.9 1.0 copy-done
  29.9 0.0 copy-start.5
  29.9 4.4 %qkv.1 = (bf16[256,2048]{1,0:T(8,128)(2,1)}, bf16[256,128]{1,0:T(8,128)(2,1)}, bf16[256,256]{1,0:T(8,128)(2,1)}) custom-call(bf16[256,2048]{1,0:T(8,128)(2,1)} %bitcast.12, f32[1,2048]{1,0:T(1,128)} %bitcast.17, bf16[2048,128]{1,0:T(8,128)(2,1)} %wq_ref.1, bf16[2048,128]{1,0:T(8,128)(2,1)} %wk_ref.2, bf16[2048,128]{1,0:T(8,128)(2,1)} %wv_ref.2, ...), custom_call_target="tpu_custom_call" | custom-call | flops 402653184 | bytes 6291456 | tf_op jit(solution)/shard_map/qkv/pallas_call | solution.py:388
  34.3 0.0 all-gather.4.cloned.1.call-update
  34.3 0.0 copy-done.2
  34.3 1.0 copy.23.wd_ref
  35.4 0.0 copy-done.3
  35.4 1.0 copy.24.wg_ref
  36.4 0.0 copy-done.5
  36.4 0.0 copy-start.4
  36.4 0.8 copy.25.extra_ref
  37.2 0.6 pad_add_fusion.place_ref
  37.7 11.1 %linear.1 = (bf16[256,128]{1,0:T(8,128)(2,1)}, f32[256,128]{1,0:T(8,128)}, bf16[128,128]{1,0:T(8,128)(2,1)}) custom-call(bf16[256,2048]{1,0:T(8,128)(2,1)} %get-tuple-element.16.normed_ref, bf16[2048,128]{1,0:T(8,128)(2,1)} %wr_ref.1, bf16[2048,128]{1,0:T(8,128)(2,1)} %wk_ref.3, bf16[2048,128]{1,0:T(8,128)(2,1)} %wv_ref.3, bf16[2048,64]{1,0:T(8,128)(2,1)} %copy.23.wd_ref, ...), custom_call_target="tpu_custom_call" | custom-call | flops 1073741824 | bytes 6291456 | tf_op jit(solution)/shard_map/linear/pallas_call | solution.py:410
  48.8 0.0 copy-done.4
  48.8 0.8 pad_maximum_fusion
  49.5 13.8 %all-gather = bf16[1536,128]{1,0:T(8,128)(2,1)} all-gather(bf16[384,128]{1,0:T(8,128)(2,1)S(1)} %pad_maximum_fusion), channel_id=2, replica_groups=mesh['z'=16,'y'=4,'tp'=8] {'y'}, dimensions={0}, use_global_device_ids=true | all-gather | bytes 491520 | tf_op jit(solution)/shard_map/all_gather | solution.py:436
  63.3 2.1 %row.1 = (bf16[128,128]{1,0:T(8,128)(2,1)}, f32[128,128]{1,0:T(8,128)}) custom-call(s32[2]{0:T(128)} %pad_add_fusion.place_ref, bf16[4,384,128]{2,1,0:T(8,128)(2,1)} %bitcast.15), custom_call_target="tpu_custom_call" | custom-call | flops 134217728 | bytes 1048576 | tf_op jit(solution)/shard_map/row/pallas_call | solution.py:437
  65.5 33.7 %all-gather.1 = bf16[2048,128]{1,0:T(8,128)(2,1)} all-gather(bf16[128,128]{1,0:T(8,128)(2,1)} %get-tuple-element.19), channel_id=3, replica_groups=mesh['z'=16,'y'=4,'tp'=8] {'z'}, dimensions={0}, use_global_device_ids=true | all-gather | bytes 557056 | tf_op jit(solution)/shard_map/all_gather | solution.py:446
  99.1 2.8 %carry.1.state_ref = bf16[128,128]{1,0:T(8,128)(2,1)} custom-call(s32[2]{0:T(128)} %pad_add_fusion.place_ref, bf16[16,128,128]{2,1,0:T(8,128)(2,1)} %bitcast.14, f32[128,128]{1,0:T(8,128)} %get-tuple-element.20.before_ref), custom_call_target="tpu_custom_call" | custom-call | flops 134217728 | bytes 1048576 | tf_op jit(solution)/shard_map/carry/pallas_call | solution.py:447
  101.9 1.9 %all-gather.4.cloned.1.call-done.kv_ref = bf16[4096,256]{1,0:T(8,128)(2,1)} async-done(((bf16[256,256]{1,0:T(8,128)(2,1)}), bf16[4096,256]{1,0:T(8,128)(2,1)}) %all-gather.4.cloned.1.call-update) | async-done | bytes 2097168 | tf_op jit(solution)/shard_map/all_gather | solution.py:409
  103.8 17.2 %attend.1 = bf16[4,272,256]{2,1,0:T(8,128)(2,1)} custom-call(s32[2]{0:T(128)} %pad_add_fusion.place_ref, bf16[4,384,128]{2,1,0:T(8,128)(2,1)} %bitcast.16, bf16[4096,256]{1,0:T(8,128)(2,1)} %all-gather.4.cloned.1.call-done.kv_ref), custom_call_target="tpu_custom_call" | custom-call | flops 6442450944 | bytes 6291456 | tf_op jit(solution)/shard_map/attend/pallas_call | solution.py:458
  120.9 4.1 %all-to-all-start.1 = ((bf16[4,272,256]{2,1,0:T(8,128)(2,1)}), bf16[4,272,256]{2,1,0:T(8,128)(2,1)S(1)}, u32[]{:S(2)}, u32[]{:S(2)}) async-start(bf16[4,272,256]{2,1,0:T(8,128)(2,1)} %attend.1), calls=%async_computation.1 | async-start | bytes 1114112 | tf_op jit(solution)/shard_map/all_to_all | solution.py:472
  125.7 7.6 %all-to-all-done.1.parts_ref = bf16[4,272,256]{2,1,0:T(8,128)(2,1)S(1)} async-done(((bf16[4,272,256]{2,1,0:T(8,128)(2,1)}), bf16[4,272,256]{2,1,0:T(8,128)(2,1)S(1)}, u32[]{:S(2)}, u32[]{:S(2)}) %all-to-all-start.1) | async-done | bytes 557088 | tf_op jit(solution)/shard_map/all_to_all | solution.py:472
  133.3 0.0 copy-start.1
  133.3 0.8 copy-done.1
  134.1 4.9 %finish.1 = bf16[256,2048]{1,0:T(8,128)(2,1)} custom-call(f32[1]{0:T(128)S(6)} %copy.26.lam_ref, bf16[4,272,256]{2,1,0:T(8,128)(2,1)} %copy-done.1, f32[1,128]{1,0:T(1,128)} %bitcast.19, bf16[256,128]{1,0:T(8,128)(2,1)} %get-tuple-element.22.qh_ref, f32[256,128]{1,0:T(8,128)} %get-tuple-element.23.ol_ref, bf16[128,128]{1,0:T(8,128)(2,1)} %carry.1.state_ref, ...), custom_call_target="tpu_custom_call" | custom-call | flops 268435456 | bytes 4194304 | tf_op jit(solution)/shard_map/finish/pallas_call | solution.py:473
  139.1 20.5 %all_to_all.15 = bf16[8,32,2048]{2,1,0:T(8,128)(2,1)S(1)} all-to-all(bf16[8,32,2048]{2,1,0:T(8,128)(2,1)} %bitcast.13), channel_id=1, replica_groups=mesh['z'=16,'y'=4,'tp'=8] {'tp'}, dimensions={0} | all-to-all | bytes 2097152 | tf_op jit(solution)/shard_map/all_to_all | solution.py:492
  159.6 0.8 reduce_sum.12
  (2 shorter events, 0.0 us)
Async XLA Ops:
  6.5 6.5 %copy-start.6 = (f32[64]{0:T(128)S(1)}, f32[64]{0:T(128)}, u32[]{:S(2)}) copy-start(f32[64]{0:T(128)} %param.38) | copy-start | bytes 772
  6.5 7.2 %copy-start.7 = (f32[64]{0:T(128)S(1)}, f32[64]{0:T(128)}, u32[]{:S(2)}) copy-start(f32[64]{0:T(128)} %param.39) | copy-start | bytes 772
  8.6 25.8 %copy-start.2 = (bf16[2048,64]{0,1:T(8,128)(2,1)S(1)}, bf16[2048,64]{0,1:T(8,128)(2,1)}, u32[]{:S(2)}) copy-start(bf16[2048,64]{0,1:T(8,128)(2,1)} %param.27) | copy-start | bytes 786436
  8.6 20.4 %all-to-all-start = ((bf16[8,32,2048]{2,1,0:T(8,128)(2,1)}), bf16[8,32,2048]{2,1,0:T(8,128)(2,1)S(1)}, u32[]{:S(2)}, u32[]{:S(2)}) async-start(bf16[8,32,2048]{2,1,0:T(8,128)(2,1)} %broadcast_in_dim.3), calls=%async_computation | async-start | bytes 2097152 | tf_op jit(solution)/shard_map/all_to_all | solution.py:354
  13.0 22.4 %copy-start.3 = (bf16[2048,64]{0,1:T(8,128)(2,1)S(1)}, bf16[2048,64]{0,1:T(8,128)(2,1)}, u32[]{:S(2)}) copy-start(bf16[2048,64]{0,1:T(8,128)(2,1)} %param.28) | copy-start | bytes 786436
  13.0 90.8 %all-gather.4.cloned.1.call-start = ((), (), s32[]{:S(2)}) async-start(), calls=%async_computation.3 | async-start | bytes 2228224 | tf_op jit(solution)/shard_map/all_gather | solution.py:409
  28.9 1.0 copy-start
  29.9 6.4 %copy-start.5 = (f32[256,2]{0,1:T(2,128)S(1)}, f32[256,2]{0,1:T(2,128)}, u32[]{:S(2)}) copy-start(f32[256,2]{0,1:T(2,128)} %param.33) | copy-start | bytes 6148
  36.4 12.4 %copy-start.4 = (bf16[256,128]{1,0:T(8,128)(2,1)S(1)}, bf16[256,128]{1,0:T(8,128)(2,1)}, u32[]{:S(2)}) copy-start(bf16[256,128]{1,0:T(8,128)(2,1)} %get-tuple-element.15) | copy-start | bytes 196612
  120.9 12.4 %all-to-all-start.1 = ((bf16[4,272,256]{2,1,0:T(8,128)(2,1)}), bf16[4,272,256]{2,1,0:T(8,128)(2,1)S(1)}, u32[]{:S(2)}, u32[]{:S(2)}) async-start(bf16[4,272,256]{2,1,0:T(8,128)(2,1)} %attend.1), calls=%async_computation.1 | async-start | bytes 1114112 | tf_op jit(solution)/shard_map/all_to_all | solution.py:472
  133.3 0.8 copy-start.1
Sparse Core Ops, SparseCore 0:
  34.4 69.2 all-gather.3

commit v2 on v1

--- a/solution.py
+++ b/solution.py
@@ -76,18 +76,21 @@
     return v.astype(BF16).astype(F32)
 
 
-def qkv_kernel(x_ref, gain_ref, wq_ref, wk_ref, wv_ref, qg_ref, kg_ref, normed_ref, q_ref, kv_ref):
-    rows = x_ref.shape[0]
-    step = 32
+def qkv_kernel(
+    mine_ref, other_ref, gain_ref, wq_ref, wk_ref, wv_ref, qg_ref, kg_ref, normed_ref, q_ref, kv_ref
+):
+    core = lax.axis_index("c")
+    chips, step, _ = mine_ref.shape
 
     def turn(i, carry):
-        span = pl.ds(pl.multiple_of(i * step, step), step)
-        x = x_ref[span, :].astype(F32)
-        scale = lax.rsqrt(jnp.mean(x * x, -1, keepdims=True) + NORM_EPS)
-        normed_ref[span, :] = (x * scale * gain_ref[...]).astype(BF16)
+        for source, at in ((mine_ref, 2 * i + core), (other_ref, 2 * i + 1 - core)):
+            x = source[i].astype(F32)
+            scale = lax.rsqrt(jnp.mean(x * x, -1, keepdims=True) + NORM_EPS)
+            span = pl.ds(pl.multiple_of(at * step, step), step)
+            normed_ref[span, :] = (x * scale * gain_ref[...]).astype(BF16)
         return carry
 
-    lax.fori_loop(0, rows // step, turn, 0)
+    lax.fori_loop(0, chips, turn, 0)
     normed = normed_ref[...]
 
     def map_norm(weight_ref, gain_ref):
@@ -102,6 +105,7 @@
 
 def linear_kernel(
     normed_ref,
+    q_ref,
     wr_ref,
     wk_ref,
     wv_ref,
@@ -111,11 +115,10 @@
     ru_ref,
     db_ref,
     rb_ref,
-    extra_ref,
     extra_t_ref,
     qh_ref,
     ol_ref,
-    map_ref,
+    pay_ref,
 ):
     normed = normed_ref[...]
     length = normed.shape[0]
@@ -123,13 +126,14 @@
     recept = rounded(dot(normed, wr_ref[...]))
     key = rounded(dot(normed, wk_ref[...]))
     value = rounded(dot(normed, wv_ref[...]))
-    decay_low = dot(normed, wd_ref[...]).astype(BF16)
-    rate_low = dot(normed, wg_ref[...]).astype(BF16)
+    decay_low = dot_nt(normed, wd_ref[...]).astype(BF16)
+    rate_low = dot_nt(normed, wg_ref[...]).astype(BF16)
     log_chan = -jnp.exp(db_ref[...] + jnp.tanh(dot(decay_low, du_ref[...])))
     gate = jax.nn.sigmoid(rb_ref[...] + jnp.tanh(dot(rate_low, ru_ref[...])))
     unit = key * lax.rsqrt(half_sums(key * key) + NORM_EPS)
-    extra = extra_ref[...]
-    head_step = jnp.where(low, extra[:, 0:1], extra[:, 1:2])
+    head_step = jnp.concatenate(
+        [jnp.broadcast_to(extra_t_ref[h : h + 1, :], (HALF, length)) for h in range(2)], axis=0
+    ).T
     row = lax.broadcasted_iota(jnp.int32, (length, length), 0)
     col = lax.broadcasted_iota(jnp.int32, (length, length), 1)
     incl = row >= col
@@ -203,7 +207,8 @@
     ol_ref[...] = jnp.where(low, outs[1], outs[0])
     r128 = lax.broadcasted_iota(jnp.int32, (LANES, LANES), 0)
     c128 = lax.broadcasted_iota(jnp.int32, (LANES, LANES), 1)
-    map_ref[...] = (
+    pay_ref[:length, :] = q_ref[...]
+    pay_ref[length:, :] = (
         maps[0] + maps[1] + jnp.where(r128 == c128, jnp.exp(ending) - 1.0, 0.0)
     ).astype(BF16)
 
@@ -219,8 +224,8 @@
     return dot3(jnp.where(same, later, 0.0), earlier) + jnp.where(same, 0.0, later)
 
 
-def row_kernel(place_ref, maps_ref, total_ref, before_ref):
-    y = place_ref[1]
+def row_kernel(maps_ref, total_ref, before_ref):
+    y = lax.axis_index("y")
     same, eye = map_masks()
     peers, rows, _ = maps_ref.shape
     so_far = eye
@@ -233,8 +238,8 @@
     total_ref[...] = (so_far - eye).astype(BF16)
 
 
-def carry_kernel(place_ref, totals_ref, before_ref, state_ref):
-    z = place_ref[0]
+def carry_kernel(totals_ref, before_ref, state_ref):
+    z = lax.axis_index("z")
     same, eye = map_masks()
     peers = totals_ref.shape[0]
     level = [
@@ -246,48 +251,58 @@
     state_ref[...] = jnp.where(same, 0.0, full).astype(BF16)
 
 
-def attend_kernel(place_ref, q_ref, kv_ref, out_ref, top_ref, acc_ref, wide_ref):
-    z = place_ref[0]
-    y = place_ref[1]
+def attend_kernel(q_ref, kv_ref, out_ref, top_ref, acc_ref, wide_ref):
+    z = lax.axis_index("z")
+    y = lax.axis_index("y")
     rows_q = q_ref.shape[0]
-    blk = 256
-    span = 1024
+    blk = top_ref.shape[1]
+    span = 4 * blk
     low = low_lanes()
     wide_ref[:, :LANES] = kv_ref[:, LANES:]
     wide_ref[:, LANES:] = jnp.ones((kv_ref.shape[0], LANES), BF16)
     top_ref[...] = jnp.full(top_ref.shape, FLOOR, F32)
     acc_ref[...] = jnp.zeros(acc_ref.shape, F32)
 
-    def step(start, masked):
+    def step(index, masked):
+        start = pl.multiple_of(index * span, span)
         keys = kv_ref[pl.ds(start, span), :LANES]
         wide = wide_ref[pl.ds(start, span), :]
-        for t in range(rows_q):
-            q = q_ref[t, :blk, :]
+
+        def scores(at):
+            own = low if at % 2 == 0 else jnp.logical_not(low)
+            q = q_ref[at // 2, :blk, :]
+            return dot_nt(jnp.where(own, q, jnp.zeros_like(q)), keys)
+
+        if masked:
+            row = lax.broadcasted_iota(jnp.int32, (blk, span), 0)
+            col = lax.broadcasted_iota(jnp.int32, (blk, span), 1)
+            k_place = (jnp.right_shift(col, 8) + index * 4) * rows_q + y
+            behind = (k_place - z * rows_q) * blk + jnp.bitwise_and(col, blk - 1) - row
+        ahead = [scores(at) for at in range(1)]
+        for at in range(2 * rows_q):
+            if at + 1 < 2 * rows_q:
+                ahead.append(scores(at + 1))
+            s = ahead.pop(0) * SCORE
             if masked:
-                row = lax.broadcasted_iota(jnp.int32, (blk, span), 0) + (z * rows_q + t) * blk
-                col = lax.broadcasted_iota(jnp.int32, (blk, span), 1)
-                k_place = (jnp.right_shift(col, 8) + jnp.right_shift(start, 8)) * rows_q + y
-                allowed = row >= k_place * blk + jnp.bitwise_and(col, blk - 1)
-            for m in range(2):
-                own = low if m == 0 else jnp.logical_not(low)
-                s = dot_nt(jnp.where(own, q, jnp.zeros_like(q)), keys) * SCORE
-                if masked:
-                    s = jnp.where(allowed, s, MASKED)
-                at = 2 * t + m
-                old = top_ref[at, :, 0:1]
-                new = jnp.maximum(old, jnp.max(s, -1, keepdims=True))
-                p = jnp.exp2(s - new).astype(BF16)
-                acc_ref[at] = acc_ref[at] * jnp.exp2(old - new) + dot(p, wide)
-                top_ref[at] = jnp.broadcast_to(new, (blk, LANES))
-
-    whole = (z * blk) // span
+                s = jnp.where(behind <= (at // 2) * blk, s, MASKED)
+            if False:
+                p = jnp.exp2(s).astype(BF16)
+                acc_ref[at] = acc_ref[at] + dot(p, wide)
+                continue
+            old = top_ref[at, :, 0:1]
+            new = jnp.maximum(old, jnp.max(s, -1, keepdims=True))
+            p = jnp.exp2(s - new).astype(BF16)
+            acc_ref[at] = acc_ref[at] * jnp.exp2(old - new) + dot(p, wide)
+            top_ref[at] = jnp.broadcast_to(new, (blk, LANES))
+
+    whole = lax.div(z, 4)
 
     def turn(i, carry):
-        step(pl.multiple_of(i * span, span), False)
+        step(i, False)
         return carry
 
     lax.fori_loop(0, whole, turn, 0)
-    step(pl.multiple_of(whole * span, span), True)
+    step(whole, True)
     lane = lax.broadcasted_iota(jnp.int32, (1, LANES), 1)
     for t in range(rows_q):
         stats = jnp.zeros((blk, LANES), F32)
@@ -349,9 +364,8 @@
         ).astype(BF16)
 
 
-def copy_for_each(x, axis):
-    copies = jnp.broadcast_to(x, (lax.axis_size(axis), *x.shape))
-    return lax.all_to_all(copies, axis, split_axis=0, concat_axis=0, tiled=True)
+def swap_cores(x):
+    return lax.ppermute(x, "c", [(0, 1), (1, 0)])
 
 
 def shards(
@@ -380,11 +394,11 @@
 ):
     shape = jax.ShapeDtypeStruct
     depth = tokens.shape[1]
-    peers = lax.axis_size("tp")
+    peers = lax.axis_size("x") * lax.axis_size("c")
     length = tokens.shape[0] * peers
-    place = jnp.stack([lax.axis_index("z"), lax.axis_index("y")]).astype(jnp.int32)
     line = lambda v: v.reshape(1, -1)
-    rows = copy_for_each(tokens, "tp").reshape(length, depth)
+    mine = lax.all_gather(tokens, "x")
+    other = swap_cores(mine)
     normed, query, key_value = pl.pallas_call(
         qkv_kernel,
         out_shape=(
@@ -392,13 +406,14 @@
             shape((length, LANES), BF16),
             shape((length, 2 * LANES), BF16),
         ),
-        in_specs=[vmem()] * 7,
+        in_specs=[vmem()] * 8,
         out_specs=(vmem(),) * 3,
         compiler_params=params(),
         cost_estimate=cost(2 * length * depth * 384, 6 << 20),
         name="qkv",
     )(
-        rows,
+        mine,
+        other,
         line(norm_gain),
         attn_query,
         attn_key,
@@ -407,12 +422,12 @@
         line(jnp.tile(key_gain, 2)),
     )
     all_kv = lax.all_gather(key_value, "z", axis=0, tiled=True)
-    reader, local_out, state_map = pl.pallas_call(
+    reader, local_out, payload = pl.pallas_call(
         linear_kernel,
         out_shape=(
             shape((length, LANES), BF16),
             shape((length, LANES), F32),
-            shape((LANES, LANES), BF16),
+            shape((length + LANES, LANES), BF16),
         ),
         in_specs=[vmem()] * 12,
         out_specs=(vmem(),) * 3,
@@ -421,44 +436,44 @@
         name="linear",
     )(
         normed,
+        query,
         recept_weight,
         key_weight,
         value_weight,
-        decay_down_weight,
-        rate_down,
+        decay_down_weight.T,
+        rate_down.T,
         decay_up,
         rate_up,
         line(decay_base),
         line(rate_base),
-        decay_extra,
         decay_extra.T,
     )
-    gathered = lax.all_gather(jnp.concatenate([query, state_map], axis=0), "y")
+    gathered = lax.all_gather(payload, "y")
     total, before = pl.pallas_call(
         row_kernel,
         out_shape=(shape((LANES, LANES), BF16), shape((LANES, LANES), F32)),
-        in_specs=[smem(), vmem()],
+        in_specs=[vmem()],
         out_specs=(vmem(),) * 2,
         compiler_params=params(),
         cost_estimate=cost(1 << 27, 1 << 20),
         name="row",
-    )(place, gathered)
+    )(gathered)
     totals = lax.all_gather(total, "z")
     state = pl.pallas_call(
         carry_kernel,
         out_shape=shape((LANES, LANES), BF16),
-        in_specs=[smem(), vmem(), vmem()],
+        in_specs=[vmem(), vmem()],
         out_specs=vmem(),
         compiler_params=params(),
         cost_estimate=cost(1 << 27, 1 << 20),
         name="carry",
-    )(place, totals, before)
+    )(totals, before)
     all_kv, state = lax.optimization_barrier((all_kv, state))
     rows_q = gathered.shape[0]
     partial = pl.pallas_call(
         attend_kernel,
         out_shape=shape((rows_q, length + STATS, 2 * LANES), BF16),
-        in_specs=[smem(), vmem(), vmem()],
+        in_specs=[vmem(), vmem()],
         out_specs=vmem(),
         scratch_shapes=[
             pltpu.VMEM((2 * rows_q, length, LANES), F32),
@@ -468,7 +483,7 @@
         compiler_params=params(),
         cost_estimate=cost(4 * rows_q * length * all_kv.shape[0] * 384, 6 << 20),
         name="attend",
-    )(place, gathered, all_kv)
+    )(gathered, all_kv)
     parts = lax.all_to_all(partial, "y", split_axis=0, concat_axis=0, tiled=True)
     share = pl.pallas_call(
         finish_kernel,
@@ -490,41 +505,47 @@
         out_attn,
     )
     arrived = lax.all_to_all(
-        share.reshape(peers, length // peers, depth), "tp", split_axis=0, concat_axis=0, tiled=True
+        share.reshape(peers, length // peers, depth),
+        ("x", "c"),
+        split_axis=0,
+        concat_axis=0,
+        tiled=True,
     )
     return arrived.astype(F32).sum(axis=0).astype(BF16)
 
 
 def solution(mesh):
-    torus = Mesh(mesh.devices.reshape(16, 4, mesh.shape["tp"]), ("z", "y", "tp"))
+    torus = Mesh(mesh.devices.reshape(16, 4, 4, 2), ("z", "y", "x", "c"))
     seq = ("z", "y")
+    tp = ("x", "c")
+    every = P(seq + tp, None)
     return jax.shard_map(
         shards,
         mesh=torus,
         in_specs=(
-            P(("z", "y", "tp"), None),
+            every,
             P(),
-            P(None, "tp"),
-            P(None, "tp"),
-            P(None, "tp"),
+            P(None, tp),
+            P(None, tp),
+            P(None, tp),
             P(),
             P(),
-            P(None, "tp"),
-            P(None, "tp"),
-            P("tp"),
-            P("tp"),
-            P(seq, "tp"),
-            P("tp"),
-            P(None, "tp"),
-            P(None, "tp"),
-            P(None, "tp"),
+            P(None, tp),
+            P(None, tp),
+            P(tp),
+            P(tp),
+            P(seq, tp),
+            P(tp),
+            P(None, tp),
+            P(None, tp),
+            P(None, tp),
             P(),
             P(),
-            P("tp"),
+            P(tp),
             P(),
-            P("tp", None),
-            P("tp", None),
+            P(tp, None),
+            P(tp, None),
         ),
-        out_specs=P(("z", "y", "tp"), None),
+        out_specs=every,
         check_vma=False,
     )

time: 168 us -> 164 us (0.976)
  blocking collectives: 68 us -> 83.9 us
  waiting for transfers between devices: 24.1 us -> 13.2 us
  local copies, waits for them, and re-layouts: 7.91 us -> 4.17 us
  starting transfers between devices: 8.58 us -> 5.75 us
    all_gather x1 -> x2, blocking collectives: 13.8 us -> 28.4 us  [the longest x1 15.1 us: shards(): gathered = lax.all_gather(payload, 'y')]
    all_to_all x1 -> x0, waiting for transfers between devices: 14.6 us -> none  [copy_for_each(): return lax.all_to_all(copies, axis, split_axis=0, concat_axis=0, tiled=True)]
    all_to_all x1 -> x0, starting transfers between devices: 4.43 us -> none  [copy_for_each(): return lax.all_to_all(copies, axis, split_axis=0, concat_axis=0, tiled=True)]
    all_gather x1, waiting for transfers between devices: 1.88 us -> 5.59 us  [shards(): all_kv = lax.all_gather(key_value, 'z', axis=0, tiled=True)]
    unnamed x19 -> x6, local copies, waits for them, and re-layouts: 4.65 us -> 1.62 us
    broadcast_in_dim x1 -> x0, local copies, waits for them, and re-layouts: 2.03 us -> none  [copy_for_each(): copies = jnp.broadcast_to(x, (lax.axis_size(axis), *x.shape))]
    ppermute x0 -> x1, starting transfers between devices: none -> 1.91 us  [swap_cores(): return lax.ppermute(x, 'c', [(0, 1), (1, 0)])]
  transfers between devices with their start and end apart: 3 -> 3, of which waited for: 3 -> 2; matrix products, arithmetic and copies ran while one was open for 3% -> 2% of each run, Pallas kernels for 10% -> 10%
where the time goes in v2:
time: 164 us; the launch traced here: 163 us
  blocking collectives  83.9 us (51%)
  Pallas kernels  41.1 us (25%)
  between operations  14.1 us (9%)
  waiting for transfers between devices  13.2 us (8%)
  starting transfers between devices  5.75 us (4%)
  local copies, waits for them, and re-layouts  4.17 us (3%)
    all_gather x1, blocking collectives, shards(): totals = lax.all_gather(total, 'z')  35 us
    all_to_all x1, blocking collectives, shards(): lax.all_to_all(share.reshape(peers, length // peers, depth), ('x', 'c'),...  20.5 us
    pallas_call x1, Pallas kernels, shards(): pl.pallas_call(attend_kernel, out_shape=shape((rows_q, length + STATS, 2...  16.3 us
    all_gather x1, blocking collectives, shards(): gathered = lax.all_gather(payload, 'y')  15.1 us
    all_gather x1, blocking collectives, shards(): mine = lax.all_gather(tokens, 'x')  13.3 us
    pallas_call x1, Pallas kernels, shards(): pl.pallas_call(linear_kernel, out_shape=(shape((length, LANES), BF16), sh...  11 us
    all_to_all x1, waiting for transfers between devices, shards(): lax.all_to_all(partial, 'y', split_axis=0, concat_axis=0, tiled=True)  7.61 us
    all_gather x1, waiting for transfers between devices, shards(): all_kv = lax.all_gather(key_value, 'z', axis=0, tiled=True)  5.59 us
  transfers between devices with their start and end apart: 3, of which 2 were waited for; matrix products, arithmetic and copies ran while one was open for 2% of the time, Pallas kernels for 10%

profile of v2, /device:TPU:480, one launch (start us, length us, event | category | flops | bytes accessed | tf_op | source)
XLA Modules:
  0.0 163.0 jit_solution(14373515833627709)
XLA Ops:
  6.5 0.0 all-gather.5.cloned.1.call-start
  6.5 13.3 %all-gather = bf16[128,2048]{1,0:T(8,128)(2,1)S(1)} all-gather(bf16[32,2048]{1,0:T(8,128)(2,1)} %param.22), channel_id=2, replica_groups=mesh['z'=16,'y'=4,'x'=4,'c'=2] {'x'}, dimensions={0}, use_global_device_ids=true | all-gather | bytes 655360 | tf_op jit(solution)/shard_map/all_gather | solution.py:400
  19.9 0.0 copy-start.1
  19.9 1.9 %collective-permute-start = (bf16[4,32,2048]{2,1,0:T(8,128)(2,1)S(1)}, bf16[4,32,2048]{2,1,0:T(8,128)(2,1)S(1)}, u32[]{:S(2)}, u32[]{:S(2)}) collective-permute-start(bf16[4,32,2048]{2,1,0:T(8,128)(2,1)S(1)} %bitcast.13), channel_id=1, source_target_pairs={{0,1},{1,0},{2,3},{3,2},{4,5},{5,4},{6,7},{7,6},{8,9},{9,8},{10,11... | collective-permute-start | bytes 1572872 | tf_op jit(solution)/shard_map/ppermute | solution.py:368
  21.8 0.7 tile.4
  22.5 0.6 reshape_tile.6.qg_ref
  23.1 0.7 tile.5
  23.8 0.6 reshape_tile.7.kg_ref
  24.3 0.0 collective-permute-done.other_ref
  24.3 0.0 copy-start.2
  24.3 0.0 copy-done.1
  24.3 0.8 copy-done.2
  25.1 4.0 %qkv.1 = (bf16[256,2048]{1,0:T(8,128)(2,1)}, bf16[256,128]{1,0:T(8,128)(2,1)}, bf16[256,256]{1,0:T(8,128)(2,1)}) custom-call(bf16[4,32,2048]{2,1,0:T(8,128)(2,1)} %bitcast.14, bf16[4,32,2048]{2,1,0:T(8,128)(2,1)} %copy-done.2, f32[1,2048]{1,0:T(1,128)} %bitcast.18, bf16[2048,128]{1,0:T(8,128)(2,1)} %wq_ref.1, bf16[2048,128]{1,0:T(8,128)(2,1)} %wk_ref.2, ...), custom_call_target="tpu_custom_call" | custom-call | flops 402653184 | bytes 6291456 | tf_op jit(solution)/shard_map/qkv/pallas_call | solution.py:402
  29.1 0.0 all-gather.5.cloned.1.call-update
  29.1 11.0 %linear.1 = (bf16[256,128]{1,0:T(8,128)(2,1)}, f32[256,128]{1,0:T(8,128)}, bf16[384,128]{1,0:T(8,128)(2,1)}) custom-call(bf16[256,2048]{1,0:T(8,128)(2,1)} %get-tuple-element.15.normed_ref, bf16[256,128]{1,0:T(8,128)(2,1)} %get-tuple-element.16.q_ref, bf16[2048,128]{1,0:T(8,128)(2,1)} %wr_ref.1, bf16[2048,128]{1,0:T(8,128)(2,1)} %wk_ref.3, ...), custom_call_target="tpu_custom_call" | custom-call | flops 1073741824 | bytes 6291456 | tf_op jit(solution)/shard_map/linear/pallas_call | solution.py:425
  40.1 15.1 %all-gather.1 = bf16[1536,128]{1,0:T(8,128)(2,1)} all-gather(bf16[384,128]{1,0:T(8,128)(2,1)} %get-tuple-element.17), channel_id=3, replica_groups=mesh['z'=16,'y'=4,'x'=4,'c'=2] {'y'}, dimensions={0}, use_global_device_ids=true | all-gather | bytes 491520 | tf_op jit(solution)/shard_map/all_gather | solution.py:451
  55.2 2.1 %row.1 = (bf16[128,128]{1,0:T(8,128)(2,1)}, f32[128,128]{1,0:T(8,128)}) custom-call(bf16[4,384,128]{2,1,0:T(8,128)(2,1)} %bitcast.16), custom_call_target="tpu_custom_call" | custom-call | flops 134217728 | bytes 1048576 | tf_op jit(solution)/shard_map/row/pallas_call | solution.py:452
  57.4 35.0 %all-gather.2 = bf16[2048,128]{1,0:T(8,128)(2,1)} all-gather(bf16[128,128]{1,0:T(8,128)(2,1)} %get-tuple-element.19), channel_id=4, replica_groups=mesh['z'=16,'y'=4,'x'=4,'c'=2] {'z'}, dimensions={0}, use_global_device_ids=true | all-gather | bytes 557056 | tf_op jit(solution)/shard_map/all_gather | solution.py:461
  92.3 2.7 %carry.1.state_ref = bf16[128,128]{1,0:T(8,128)(2,1)} custom-call(bf16[16,128,128]{2,1,0:T(8,128)(2,1)} %bitcast.15, f32[128,128]{1,0:T(8,128)} %get-tuple-element.20.before_ref), custom_call_target="tpu_custom_call" | custom-call | flops 134217728 | bytes 1048576 | tf_op jit(solution)/shard_map/carry/pallas_call | solution.py:462
  95.1 5.6 %all-gather.5.cloned.1.call-done.kv_ref = bf16[4096,256]{1,0:T(8,128)(2,1)} async-done(((bf16[256,256]{1,0:T(8,128)(2,1)}), bf16[4096,256]{1,0:T(8,128)(2,1)}) %all-gather.5.cloned.1.call-update) | async-done | bytes 2097168 | tf_op jit(solution)/shard_map/all_gather | solution.py:424
  100.6 16.3 %attend.1 = bf16[4,272,256]{2,1,0:T(8,128)(2,1)} custom-call(bf16[4,384,128]{2,1,0:T(8,128)(2,1)} %bitcast.17, bf16[4096,256]{1,0:T(8,128)(2,1)} %all-gather.5.cloned.1.call-done.kv_ref), custom_call_target="tpu_custom_call" | custom-call | flops 6442450944 | bytes 6291456 | tf_op jit(solution)/shard_map/attend/pallas_call | solution.py:473
  117.0 3.8 %all-to-all-start = ((bf16[4,272,256]{2,1,0:T(8,128)(2,1)}), bf16[4,272,256]{2,1,0:T(8,128)(2,1)S(1)}, u32[]{:S(2)}, u32[]{:S(2)}) async-start(bf16[4,272,256]{2,1,0:T(8,128)(2,1)} %attend.1), calls=%async_computation | async-start | bytes 1114112 | tf_op jit(solution)/shard_map/all_to_all | solution.py:487
  121.5 7.6 %all-to-all-done.parts_ref = bf16[4,272,256]{2,1,0:T(8,128)(2,1)S(1)} async-done(((bf16[4,272,256]{2,1,0:T(8,128)(2,1)}), bf16[4,272,256]{2,1,0:T(8,128)(2,1)S(1)}, u32[]{:S(2)}, u32[]{:S(2)}) %all-to-all-start) | async-done | bytes 557088 | tf_op jit(solution)/shard_map/all_to_all | solution.py:487
  129.1 0.0 copy-start
  129.1 0.8 copy-done
  129.9 4.9 %finish.1 = bf16[256,2048]{1,0:T(8,128)(2,1)} custom-call(f32[1]{0:T(128)S(6)} %copy.23.lam_ref, bf16[4,272,256]{2,1,0:T(8,128)(2,1)} %copy-done, f32[1,128]{1,0:T(1,128)} %bitcast.19, bf16[256,128]{1,0:T(8,128)(2,1)} %get-tuple-element.22.qh_ref, f32[256,128]{1,0:T(8,128)} %get-tuple-element.23.ol_ref, bf16[128,128]{1,0:T(8,128)(2,1)} %carry.1.state_ref, ...), custom_call_target="tpu_custom_call" | custom-call | flops 268435456 | bytes 4194304 | tf_op jit(solution)/shard_map/finish/pallas_call | solution.py:488
  134.9 20.5 %all_to_all.10 = bf16[8,32,2048]{2,1,0:T(8,128)(2,1)S(1)} all-to-all(bf16[8,32,2048]{2,1,0:T(8,128)(2,1)} %bitcast.12), channel_id=1, replica_groups=mesh['z'=16,'y'=4,'x'=4,'c'=2] {'x','c'}, dimensions={0} | all-to-all | bytes 2097152 | tf_op jit(solution)/shard_map/all_to_all | solution.py:507
  155.3 0.8 reduce_sum.12
Async XLA Ops:
  6.5 94.1 %all-gather.5.cloned.1.call-start = ((), (), s32[]{:S(2)}) async-start(), calls=%async_computation.2 | async-start | bytes 2228224 | tf_op jit(solution)/shard_map/all_gather | solution.py:424
  19.9 4.5 %copy-start.1 = (bf16[128,2048]{1,0:T(8,128)(2,1)}, bf16[128,2048]{1,0:T(8,128)(2,1)S(1)}, u32[]{:S(2)}) copy-start(bf16[128,2048]{1,0:T(8,128)(2,1)S(1)} %all-gather) | copy-start | bytes 1572868
  19.9 4.5 %collective-permute-start = (bf16[4,32,2048]{2,1,0:T(8,128)(2,1)S(1)}, bf16[4,32,2048]{2,1,0:T(8,128)(2,1)S(1)}, u32[]{:S(2)}, u32[]{:S(2)}) collective-permute-start(bf16[4,32,2048]{2,1,0:T(8,128)(2,1)S(1)} %bitcast.13), channel_id=1, source_target_pairs={{0,1},{1,0},{2,3},{3,2},{4,5},{5,4},{6,7},{7,6},{8,9},{9,8},{10,11... | collective-permute-start | bytes 1572872 | tf_op jit(solution)/shard_map/ppermute | solution.py:368
  24.3 0.8 copy-start.2
  117.0 12.1 %all-to-all-start = ((bf16[4,272,256]{2,1,0:T(8,128)(2,1)}), bf16[4,272,256]{2,1,0:T(8,128)(2,1)S(1)}, u32[]{:S(2)}, u32[]{:S(2)}) async-start(bf16[4,272,256]{2,1,0:T(8,128)(2,1)} %attend.1), calls=%async_computation | async-start | bytes 1114112 | tf_op jit(solution)/shard_map/all_to_all | solution.py:487
  129.1 0.8 copy-start
Sparse Core Ops, SparseCore 0:
  29.2 71.3 all-gather.4

commit v3 on v2

--- a/solution.py
+++ b/solution.py
@@ -19,7 +19,6 @@
 FLOOR = -1e29
 MASKED = -1e30
 STATS = 16
-VMEM_LIMIT = 56 * 1024 * 1024
 
 
 def vmem():
@@ -30,8 +29,8 @@
     return pl.BlockSpec(memory_space=pltpu.SMEM)
 
 
-def params():
-    return pltpu.CompilerParams(vmem_limit_bytes=VMEM_LIMIT)
+def params(mib):
+    return pltpu.CompilerParams(vmem_limit_bytes=mib << 20)
 
 
 def cost(flops, size):
@@ -251,69 +250,80 @@
     state_ref[...] = jnp.where(same, 0.0, full).astype(BF16)
 
 
-def attend_kernel(q_ref, kv_ref, out_ref, top_ref, acc_ref, wide_ref):
+def attend_kernel(q_ref, kv_hbm, out_ref, top_ref, acc_ref, kv_ref, wide_ref, sems):
     z = lax.axis_index("z")
     y = lax.axis_index("y")
     rows_q = q_ref.shape[0]
     blk = top_ref.shape[1]
-    span = 4 * blk
+    group = 4
+    span = group * blk
     low = low_lanes()
-    wide_ref[:, :LANES] = kv_ref[:, LANES:]
-    wide_ref[:, LANES:] = jnp.ones((kv_ref.shape[0], LANES), BF16)
-    top_ref[...] = jnp.full(top_ref.shape, FLOOR, F32)
-    acc_ref[...] = jnp.zeros(acc_ref.shape, F32)
-
-    def step(index, masked):
-        start = pl.multiple_of(index * span, span)
-        keys = kv_ref[pl.ds(start, span), :LANES]
-        wide = wide_ref[pl.ds(start, span), :]
+    whole = lax.div(z, group)
+
+    def fetch(index):
+        at = pl.ds(pl.multiple_of(index * span, span), span)
+        return pltpu.make_async_copy(kv_hbm.at[at, :], kv_ref.at[at, :], sems.at[index])
+
+    fetch(whole).start()
+
+    def begin(i, carry):
+        fetch(i).start()
+        return carry
+
+    lax.fori_loop(0, whole, begin, 0)
+    wide_ref[:, LANES:] = jnp.ones((span, LANES), BF16)
+
+    def step(index, last):
+        fetch(index).wait()
+        at_keys = pl.ds(pl.multiple_of(index * span, span), span)
+        keys = kv_ref[at_keys, :LANES]
+        wide_ref[:, :LANES] = kv_ref[at_keys, LANES:]
+        wide = wide_ref[...]
 
         def scores(at):
             own = low if at % 2 == 0 else jnp.logical_not(low)
             q = q_ref[at // 2, :blk, :]
             return dot_nt(jnp.where(own, q, jnp.zeros_like(q)), keys)
 
-        if masked:
+        if last:
             row = lax.broadcasted_iota(jnp.int32, (blk, span), 0)
             col = lax.broadcasted_iota(jnp.int32, (blk, span), 1)
-            k_place = (jnp.right_shift(col, 8) + index * 4) * rows_q + y
+            k_place = (jnp.right_shift(col, 8) + index * group) * rows_q + y
             behind = (k_place - z * rows_q) * blk + jnp.bitwise_and(col, blk - 1) - row
-        ahead = [scores(at) for at in range(1)]
+        ahead = scores(0)
         for at in range(2 * rows_q):
+            s = ahead * SCORE
             if at + 1 < 2 * rows_q:
-                ahead.append(scores(at + 1))
-            s = ahead.pop(0) * SCORE
-            if masked:
+                ahead = scores(at + 1)
+            if last:
                 s = jnp.where(behind <= (at // 2) * blk, s, MASKED)
-            if False:
-                p = jnp.exp2(s).astype(BF16)
-                acc_ref[at] = acc_ref[at] + dot(p, wide)
-                continue
-            old = top_ref[at, :, 0:1]
-            new = jnp.maximum(old, jnp.max(s, -1, keepdims=True))
-            p = jnp.exp2(s - new).astype(BF16)
-            acc_ref[at] = acc_ref[at] * jnp.exp2(old - new) + dot(p, wide)
+                new = jnp.maximum(jnp.max(s, -1, keepdims=True), FLOOR)
+                acc_ref[at] = dot(jnp.exp2(s - new).astype(BF16), wide)
+            else:
+                old = top_ref[at, :, 0:1]
+                new = jnp.maximum(old, jnp.max(s, -1, keepdims=True))
+                p = jnp.exp2(s - new).astype(BF16)
+                acc_ref[at] = acc_ref[at] * jnp.exp2(old - new) + dot(p, wide)
             top_ref[at] = jnp.broadcast_to(new, (blk, LANES))
 
-    whole = lax.div(z, 4)
+    step(whole, True)
 
     def turn(i, carry):
         step(i, False)
         return carry
 
     lax.fori_loop(0, whole, turn, 0)
-    step(whole, True)
     lane = lax.broadcasted_iota(jnp.int32, (1, LANES), 1)
     for t in range(rows_q):
         stats = jnp.zeros((blk, LANES), F32)
         for m in range(2):
             at = 2 * t + m
             acc = acc_ref[at]
-            weight = acc[:, LANES : LANES + 1]
+            weight = acc[:, LANES:]
             seen = weight > 0.0
             safe = jnp.where(seen, weight, 1.0)
             out_ref[t, :blk, m * LANES : (m + 1) * LANES] = (acc[:, :LANES] / safe).astype(BF16)
-            lse = jnp.where(seen, top_ref[at, :, 0:1] + jnp.log2(safe), MASKED)
+            lse = jnp.where(seen, top_ref[at] + jnp.log2(safe), MASKED)
             high = rounded(lse)
             mid = rounded(lse - high)
             tail = rounded(lse - high - mid)
@@ -408,7 +418,7 @@
         ),
         in_specs=[vmem()] * 8,
         out_specs=(vmem(),) * 3,
-        compiler_params=params(),
+        compiler_params=params(12),
         cost_estimate=cost(2 * length * depth * 384, 6 << 20),
         name="qkv",
     )(
@@ -431,7 +441,7 @@
         ),
         in_specs=[vmem()] * 12,
         out_specs=(vmem(),) * 3,
-        compiler_params=params(),
+        compiler_params=params(20),
         cost_estimate=cost(2 * length * depth * 1024, 6 << 20),
         name="linear",
     )(
@@ -454,7 +464,7 @@
         out_shape=(shape((LANES, LANES), BF16), shape((LANES, LANES), F32)),
         in_specs=[vmem()],
         out_specs=(vmem(),) * 2,
-        compiler_params=params(),
+        compiler_params=params(6),
         cost_estimate=cost(1 << 27, 1 << 20),
         name="row",
     )(gathered)
@@ -464,7 +474,7 @@
         out_shape=shape((LANES, LANES), BF16),
         in_specs=[vmem(), vmem()],
         out_specs=vmem(),
-        compiler_params=params(),
+        compiler_params=params(6),
         cost_estimate=cost(1 << 27, 1 << 20),
         name="carry",
     )(totals, before)
@@ -473,14 +483,16 @@
     partial = pl.pallas_call(
         attend_kernel,
         out_shape=shape((rows_q, length + STATS, 2 * LANES), BF16),
-        in_specs=[vmem(), vmem()],
+        in_specs=[vmem(), pl.BlockSpec(memory_space=pltpu.HBM)],
         out_specs=vmem(),
         scratch_shapes=[
             pltpu.VMEM((2 * rows_q, length, LANES), F32),
             pltpu.VMEM((2 * rows_q, length, 2 * LANES), F32),
-            pltpu.VMEM((all_kv.shape[0], 2 * LANES), BF16),
+            pltpu.VMEM(all_kv.shape, BF16),
+            pltpu.VMEM((4 * length, 2 * LANES), BF16),
+            pltpu.SemaphoreType.DMA((all_kv.shape[0] // (4 * length),)),
         ],
-        compiler_params=params(),
+        compiler_params=params(62),
         cost_estimate=cost(4 * rows_q * length * all_kv.shape[0] * 384, 6 << 20),
         name="attend",
     )(gathered, all_kv)
@@ -490,7 +502,7 @@
         out_shape=shape((length, depth), BF16),
         in_specs=[smem()] + [vmem()] * 8,
         out_specs=vmem(),
-        compiler_params=params(),
+        compiler_params=params(12),
         cost_estimate=cost(2 * length * depth * 256, 4 << 20),
         name="finish",
     )(

time: 164 us -> 162 us (0.988)
  Pallas kernels: 41.1 us -> 31.2 us
  waiting for transfers between devices: 13.2 us -> 20.4 us
  blocking collectives: 83.9 us -> 80.2 us
  local copies, waits for them, and re-layouts: 4.17 us -> 7.44 us
    all_gather x1, waiting for transfers between devices: 5.59 us -> 12.4 us  [shards(): all_kv = lax.all_gather(key_value, 'z', axis=0, tiled=True)]
    unnamed x6 -> x38, local copies, waits for them, and re-layouts: 1.62 us -> 5.96 us
    pallas_call x1, Pallas kernels: 11 us -> 8.42 us  [shards(): pl.pallas_call(linear_kernel, out_shape=(shape((length, LANES), BF16), sh...]
    pallas_call x1, Pallas kernels: 4.92 us -> 2.47 us  [shards(): pl.pallas_call(finish_kernel, out_shape=shape((length, depth), BF16), in_...]
    all_gather x1, blocking collectives: 15.1 us -> 13 us  [shards(): gathered = lax.all_gather(payload, 'y')]
    all_gather x1, blocking collectives: 35 us -> 32.9 us  [shards(): totals = lax.all_gather(total, 'z')]
    pallas_call x1, Pallas kernels: 3.97 us -> 2.28 us  [shards(): pl.pallas_call(qkv_kernel, out_shape=(shape((length, depth), BF16), shape...]
    pallas_call x1, Pallas kernels: 2.73 us -> 1.09 us  [shards(): pl.pallas_call(carry_kernel, out_shape=shape((LANES, LANES), BF16), in_sp...]
  transfers between devices with their start and end apart: 3 -> 3, of which waited for: 2 -> 3; matrix products, arithmetic and copies ran while one was open for 2% -> 1% of each run, Pallas kernels for 10% -> 6%
where the time goes in v3:
time: 162 us; the launch traced here: 161 us
  blocking collectives  80.2 us (50%)
  Pallas kernels  31.2 us (19%)
  waiting for transfers between devices  20.4 us (13%)
  between operations  14.2 us (9%)
  local copies, waits for them, and re-layouts  7.44 us (5%)
  starting transfers between devices  6.91 us (4%)
    all_gather x1, blocking collectives, shards(): totals = lax.all_gather(total, 'z')  32.9 us
    all_to_all x1, blocking collectives, shards(): lax.all_to_all(share.reshape(peers, length // peers, depth), ('x', 'c'),...  20.8 us
    pallas_call x1, Pallas kernels, shards(): pl.pallas_call(attend_kernel, out_shape=shape((rows_q, length + STATS, 2...  16.4 us
    all_gather x1, blocking collectives, shards(): mine = lax.all_gather(tokens, 'x')  13.5 us
    all_gather x1, blocking collectives, shards(): gathered = lax.all_gather(payload, 'y')  13 us
    all_gather x1, waiting for transfers between devices, shards(): all_kv = lax.all_gather(key_value, 'z', axis=0, tiled=True)  12.4 us
    pallas_call x1, Pallas kernels, shards(): pl.pallas_call(linear_kernel, out_shape=(shape((length, LANES), BF16), sh...  8.42 us
    all_to_all x1, waiting for transfers between devices, shards(): lax.all_to_all(partial, 'y', split_axis=0, concat_axis=0, tiled=True)  7.61 us
  transfers between devices with their start and end apart: 3, of which 3 were waited for; matrix products, arithmetic and copies ran while one was open for 1% of the time, Pallas kernels for 6%

profile of v3, /device:TPU:480, one launch (start us, length us, event | category | flops | bytes accessed | tf_op | source)
XLA Modules:
  0.0 161.3 jit_solution(9809280567071501689)
XLA Ops:
  6.5 0.0 copy-start.17
  6.5 0.0 copy-start.18
  6.5 0.0 copy-start.16
  6.5 0.0 copy-start.9
  6.5 0.0 copy-start.14
  6.5 0.0 copy-start.15
  6.6 0.0 all-gather.5.cloned.1.call-start
  6.6 13.5 %all-gather = bf16[128,2048]{1,0:T(8,128)(2,1)S(1)} all-gather(bf16[32,2048]{1,0:T(8,128)(2,1)} %param.22), channel_id=2, replica_groups=mesh['z'=16,'y'=4,'x'=4,'c'=2] {'x'}, dimensions={0}, use_global_device_ids=true | all-gather | bytes 655360 | tf_op jit(solution)/shard_map/all_gather | solution.py:410
  20.1 1.9 %collective-permute-start = (bf16[4,32,2048]{2,1,0:T(8,128)(2,1)S(1)}, bf16[4,32,2048]{2,1,0:T(8,128)(2,1)S(1)}, u32[]{:S(2)}, u32[]{:S(2)}) collective-permute-start(bf16[4,32,2048]{2,1,0:T(8,128)(2,1)S(1)} %bitcast.13), channel_id=1, source_target_pairs={{0,1},{1,0},{2,3},{3,2},{4,5},{5,4},{6,7},{7,6},{8,9},{9,8},{10,11... | collective-permute-start | bytes 1572872 | tf_op jit(solution)/shard_map/ppermute | solution.py:378
  22.0 0.7 tile.4
  22.7 0.1 reshape_tile.6.qg_ref
  22.7 0.7 tile.5
  23.4 0.1 reshape_tile.7.kg_ref
  23.5 0.4 collective-permute-done.other_ref
  23.9 0.0 copy-start
  23.9 1.0 copy-done
  24.9 0.0 copy-start.1
  24.9 1.0 copy-done.1
  26.0 0.0 copy-start.2
  26.0 1.0 copy-done.2
  27.0 0.0 copy-start.6
  27.0 0.7 copy-done.6
  27.7 0.0 copy-start.12
  27.7 0.0 copy-start.13
  27.7 2.3 %qkv.1 = (bf16[256,2048]{1,0:T(8,128)(2,1)S(1)}, bf16[256,128]{1,0:T(8,128)(2,1)S(1)}, bf16[256,256]{1,0:T(8,128)(2,1)}) custom-call(bf16[4,32,2048]{2,1,0:T(8,128)(2,1)S(1)} %bitcast.14, bf16[4,32,2048]{2,1,0:T(8,128)(2,1)S(1)} %collective-permute-done.other_ref, f32[1,2048]{1,0:T(1,128)S(1)} %bitcast.18, bf16[2048,128]{1,0:T(8,128)(2,1)S(1)} %copy-done, ...), custom_call_target="tpu_custom_call" | custom-call | flops 402653184 | bytes 6291456 | tf_op jit(solution)/shard_map/qkv/pallas_call | solution.py:412
  30.0 0.0 all-gather.5.cloned.1.call-update
  30.0 0.0 copy-done.17
  30.0 0.0 copy-done.18
  30.0 0.0 copy-done.16
  30.0 0.0 copy-done.9
  30.0 0.0 copy-done.14
  30.1 0.0 copy-done.15
  30.1 0.0 copy-done.12
  30.1 0.0 copy-done.13
  30.1 0.0 copy-start.10
  30.1 1.0 copy-done.10
  31.1 0.0 copy-start.11
  31.1 1.0 copy-done.11
  32.2 8.4 %linear.1 = (bf16[256,128]{1,0:T(8,128)(2,1)S(1)}, f32[256,128]{1,0:T(8,128)S(1)}, bf16[384,128]{1,0:T(8,128)(2,1)S(1)}) custom-call(bf16[256,2048]{1,0:T(8,128)(2,1)S(1)} %get-tuple-element.15.normed_ref, bf16[256,128]{1,0:T(8,128)(2,1)S(1)} %get-tuple-element.16.q_ref, bf16[2048,128]{1,0:T(8,128)(2,1)S(1)} %copy-done.9, bf16[2048,128]{1,0:T(8,128)(2,1)S(1)} %copy-done.10, ...), custom_call_target="tpu_custom_call" | custom-call | flops 1073741824 | bytes 6291456 | tf_op jit(solution)/shard_map/linear/pallas_call | solution.py:435
  40.6 13.0 %all-gather.1 = bf16[1536,128]{1,0:T(8,128)(2,1)S(1)} all-gather(bf16[384,128]{1,0:T(8,128)(2,1)S(1)} %get-tuple-element.17), channel_id=3, replica_groups=mesh['z'=16,'y'=4,'x'=4,'c'=2] {'y'}, dimensions={0}, use_global_device_ids=true | all-gather | bytes 491520 | tf_op jit(solution)/shard_map/all_gather | solution.py:461
  53.6 0.0 copy-start.5
  53.6 0.5 row.1
  54.2 32.9 %all-gather.2 = bf16[2048,128]{1,0:T(8,128)(2,1)S(1)} all-gather(bf16[128,128]{1,0:T(8,128)(2,1)S(1)} %get-tuple-element.19), channel_id=4, replica_groups=mesh['z'=16,'y'=4,'x'=4,'c'=2] {'z'}, dimensions={0}, use_global_device_ids=true | all-gather | bytes 557056 | tf_op jit(solution)/shard_map/all_gather | solution.py:471
  87.1 1.1 carry.1.state_ref
  88.2 0.0 copy-start.3
  88.2 0.0 copy-start.4
  88.2 0.0 copy-start.7
  88.2 0.0 copy-start.8
  88.3 12.4 %all-gather.5.cloned.1.call-done.kv_hbm = bf16[4096,256]{1,0:T(8,128)(2,1)} async-done(((bf16[256,256]{1,0:T(8,128)(2,1)}), bf16[4096,256]{1,0:T(8,128)(2,1)}) %all-gather.5.cloned.1.call-update) | async-done | bytes 2097168 | tf_op jit(solution)/shard_map/all_gather | solution.py:434
  100.6 0.0 copy-done.5
  100.6 16.4 %attend.1 = bf16[4,272,256]{2,1,0:T(8,128)(2,1)} custom-call(bf16[4,384,128]{2,1,0:T(8,128)(2,1)} %bitcast.17, bf16[4096,256]{1,0:T(8,128)(2,1)} %all-gather.5.cloned.1.call-done.kv_hbm), custom_call_target="tpu_custom_call" | custom-call | flops 6442450944 | bytes 6291456 | tf_op jit(solution)/shard_map/attend/pallas_call | solution.py:483
  117.1 5.0 %all-to-all-start = ((bf16[4,272,256]{2,1,0:T(8,128)(2,1)}), bf16[4,272,256]{2,1,0:T(8,128)(2,1)S(1)}, u32[]{:S(2)}, u32[]{:S(2)}) async-start(bf16[4,272,256]{2,1,0:T(8,128)(2,1)} %attend.1), calls=%async_computation | async-start | bytes 1114112 | tf_op jit(solution)/shard_map/all_to_all | solution.py:499
  122.7 7.6 %all-to-all-done.parts_ref = bf16[4,272,256]{2,1,0:T(8,128)(2,1)S(1)} async-done(((bf16[4,272,256]{2,1,0:T(8,128)(2,1)}), bf16[4,272,256]{2,1,0:T(8,128)(2,1)S(1)}, u32[]{:S(2)}, u32[]{:S(2)}) %all-to-all-start) | async-done | bytes 557088 | tf_op jit(solution)/shard_map/all_to_all | solution.py:499
  130.3 0.0 copy-done.3
  130.3 0.0 copy-done.4
  130.3 0.0 copy-done.7
  130.3 0.0 copy-done.8
  130.3 2.5 %finish.1 = bf16[256,2048]{1,0:T(8,128)(2,1)S(1)} custom-call(f32[1]{0:T(128)S(6)} %copy.23.lam_ref, bf16[4,272,256]{2,1,0:T(8,128)(2,1)S(1)} %all-to-all-done.parts_ref, f32[1,128]{1,0:T(1,128)S(1)} %bitcast.19, bf16[256,128]{1,0:T(8,128)(2,1)S(1)} %get-tuple-element.22.qh_ref, f32[256,128]{1,0:T(8,128)S(1)} %get-tuple-element.23.ol_ref, ...), custom_call_target="tpu_custom_call" | custom-call | flops 268435456 | bytes 4194304 | tf_op jit(solution)/shard_map/finish/pallas_call | solution.py:500
  132.8 20.8 %all_to_all.10 = bf16[8,32,2048]{2,1,0:T(8,128)(2,1)S(1)} all-to-all(bf16[8,32,2048]{2,1,0:T(8,128)(2,1)S(1)} %bitcast.12), channel_id=1, replica_groups=mesh['z'=16,'y'=4,'x'=4,'c'=2] {'x','c'}, dimensions={0} | all-to-all | bytes 2097152 | tf_op jit(solution)/shard_map/all_to_all | solution.py:519
  153.6 0.8 reduce_sum.12
Async XLA Ops:
  6.5 23.5 %copy-start.17 = (f32[128]{0:T(128)S(1)}, f32[128]{0:T(128)}, u32[]{:S(2)}) copy-start(f32[128]{0:T(128)} %param.31) | copy-start | bytes 1540
  6.5 23.5 %copy-start.18 = (f32[128]{0:T(128)S(1)}, f32[128]{0:T(128)}, u32[]{:S(2)}) copy-start(f32[128]{0:T(128)} %param.32) | copy-start | bytes 1540
  6.5 23.5 %copy-start.16 = (f32[256,2]{0,1:T(2,128)S(1)}, f32[256,2]{0,1:T(2,128)}, u32[]{:S(2)}) copy-start(f32[256,2]{0,1:T(2,128)} %param.33) | copy-start | bytes 6148
  6.5 23.5 %copy-start.9 = (bf16[2048,128]{1,0:T(8,128)(2,1)S(1)}, bf16[2048,128]{1,0:T(8,128)(2,1)}, u32[]{:S(2)}) copy-start(bf16[2048,128]{1,0:T(8,128)(2,1)} %wr_ref.1) | copy-start | bytes 1572868
  6.5 23.5 %copy-start.14 = (bf16[64,128]{1,0:T(8,128)(2,1)S(1)}, bf16[64,128]{1,0:T(8,128)(2,1)}, u32[]{:S(2)}) copy-start(bf16[64,128]{1,0:T(8,128)(2,1)} %du_ref.1) | copy-start | bytes 49156
  6.5 23.5 %copy-start.15 = (bf16[64,128]{1,0:T(8,128)(2,1)S(1)}, bf16[64,128]{1,0:T(8,128)(2,1)}, u32[]{:S(2)}) copy-start(bf16[64,128]{1,0:T(8,128)(2,1)} %ru_ref.1) | copy-start | bytes 49156
  6.6 94.1 %all-gather.5.cloned.1.call-start = ((), (), s32[]{:S(2)}) async-start(), calls=%async_computation.2 | async-start | bytes 2228224 | tf_op jit(solution)/shard_map/all_gather | solution.py:434
  20.1 3.8 %collective-permute-start = (bf16[4,32,2048]{2,1,0:T(8,128)(2,1)S(1)}, bf16[4,32,2048]{2,1,0:T(8,128)(2,1)S(1)}, u32[]{:S(2)}, u32[]{:S(2)}) collective-permute-start(bf16[4,32,2048]{2,1,0:T(8,128)(2,1)S(1)} %bitcast.13), channel_id=1, source_target_pairs={{0,1},{1,0},{2,3},{3,2},{4,5},{5,4},{6,7},{7,6},{8,9},{9,8},{10,11... | collective-permute-start | bytes 1572872 | tf_op jit(solution)/shard_map/ppermute | solution.py:378
  23.9 1.0 copy-start
  24.9 1.0 copy-start.1
  26.0 1.0 copy-start.2
  27.0 0.7 copy-start.6
  27.7 2.4 %copy-start.12 = (bf16[2048,64]{0,1:T(8,128)(2,1)S(1)}, bf16[2048,64]{0,1:T(8,128)(2,1)}, u32[]{:S(2)}) copy-start(bf16[2048,64]{0,1:T(8,128)(2,1)} %param.27) | copy-start | bytes 786436
  27.7 2.4 %copy-start.13 = (bf16[2048,64]{0,1:T(8,128)(2,1)S(1)}, bf16[2048,64]{0,1:T(8,128)(2,1)}, u32[]{:S(2)}) copy-start(bf16[2048,64]{0,1:T(8,128)(2,1)} %param.28) | copy-start | bytes 786436
  30.1 1.0 copy-start.10
  31.1 1.0 copy-start.11
  53.6 47.0 %copy-start.5 = (bf16[1536,128]{1,0:T(8,128)(2,1)}, bf16[1536,128]{1,0:T(8,128)(2,1)S(1)}, u32[]{:S(2)}) copy-start(bf16[1536,128]{1,0:T(8,128)(2,1)S(1)} %all-gather.1) | copy-start | bytes 1179652
  88.2 42.1 %copy-start.3 = (bf16[128,2048]{1,0:T(8,128)(2,1)S(1)}, bf16[128,2048]{1,0:T(8,128)(2,1)}, u32[]{:S(2)}) copy-start(bf16[128,2048]{1,0:T(8,128)(2,1)} %wl_ref.1) | copy-start | bytes 1572868
  88.2 42.1 %copy-start.4 = (bf16[128,2048]{1,0:T(8,128)(2,1)S(1)}, bf16[128,2048]{1,0:T(8,128)(2,1)}, u32[]{:S(2)}) copy-start(bf16[128,2048]{1,0:T(8,128)(2,1)} %wa_ref.1) | copy-start | bytes 1572868
  88.2 42.1 %copy-start.7 = (f32[128]{0:T(128)S(1)}, f32[128]{0:T(128)}, u32[]{:S(2)}) copy-start(f32[128]{0:T(128)} %param.41) | copy-start | bytes 1540
  88.2 42.1 %copy-start.8 = (f32[128]{0:T(128)S(1)}, f32[128]{0:T(128)}, u32[]{:S(2)}) copy-start(f32[128]{0:T(128)} %param.34) | copy-start | bytes 1540
  117.1 13.2 %all-to-all-start = ((bf16[4,272,256]{2,1,0:T(8,128)(2,1)}), bf16[4,272,256]{2,1,0:T(8,128)(2,1)S(1)}, u32[]{:S(2)}, u32[]{:S(2)}) async-start(bf16[4,272,256]{2,1,0:T(8,128)(2,1)} %attend.1), calls=%async_computation | async-start | bytes 1114112 | tf_op jit(solution)/shard_map/all_to_all | solution.py:499
Sparse Core Ops, SparseCore 0:
  30.1 70.4 all-gather.4

commit v4 on v3

--- a/solution.py
+++ b/solution.py
@@ -260,22 +260,21 @@
     low = low_lanes()
     whole = lax.div(z, group)
 
-    def fetch(index):
-        at = pl.ds(pl.multiple_of(index * span, span), span)
-        return pltpu.make_async_copy(kv_hbm.at[at, :], kv_ref.at[at, :], sems.at[index])
-
-    fetch(whole).start()
-
     def begin(i, carry):
-        fetch(i).start()
+        for part in range(group):
+            at = pl.ds(pl.multiple_of(i * span + part * blk, blk), blk)
+            pltpu.make_async_copy(kv_hbm.at[at, :], kv_ref.at[at, :], sems.at[i]).start()
         return carry
 
+    begin(whole, 0)
     lax.fori_loop(0, whole, begin, 0)
     wide_ref[:, LANES:] = jnp.ones((span, LANES), BF16)
 
     def step(index, last):
-        fetch(index).wait()
         at_keys = pl.ds(pl.multiple_of(index * span, span), span)
+        pltpu.make_async_copy(
+            kv_hbm.at[at_keys, :], kv_ref.at[at_keys, :], sems.at[index]
+        ).wait()
         keys = kv_ref[at_keys, :LANES]
         wide_ref[:, :LANES] = kv_ref[at_keys, LANES:]
         wide = wide_ref[...]
@@ -418,7 +417,7 @@
         ),
         in_specs=[vmem()] * 8,
         out_specs=(vmem(),) * 3,
-        compiler_params=params(12),
+        compiler_params=params(61),
         cost_estimate=cost(2 * length * depth * 384, 6 << 20),
         name="qkv",
     )(

time: 162 us -> 160 us (0.988)
  local copies, waits for them, and re-layouts: 7.44 us -> 4.71 us
  Pallas kernels: 31.2 us -> 33 us
    unnamed x38 -> x36, local copies, waits for them, and re-layouts: 5.96 us -> 2.13 us
    pallas_call x1, Pallas kernels: 2.28 us -> 3.97 us  [shards(): pl.pallas_call(qkv_kernel, out_shape=(shape((length, depth), BF16), shape...]
  transfers between devices with their start and end apart: 3 -> 3, of which waited for: 3 -> 2; matrix products, arithmetic and copies ran while one was open for 1% -> 2% of each run, Pallas kernels for 6% -> 6%
where the time goes in v4:
time: 160 us
  blocking collectives  80.2 us (50%)
  Pallas kernels  33 us (21%)
  waiting for transfers between devices  20.3 us (13%)
  between operations  14.3 us (9%)
  starting transfers between devices  6.55 us (4%)
  local copies, waits for them, and re-layouts  4.71 us (3%)
    all_gather x1, blocking collectives, shards(): totals = lax.all_gather(total, 'z')  33 us
    all_to_all x1, blocking collectives, shards(): lax.all_to_all(share.reshape(peers, length // peers, depth), ('x', 'c'),...  20.6 us
    pallas_call x1, Pallas kernels, shards(): pl.pallas_call(attend_kernel, out_shape=shape((rows_q, length + STATS, 2...  16.5 us
    all_gather x1, blocking collectives, shards(): mine = lax.all_gather(tokens, 'x')  13.5 us
    all_gather x1, blocking collectives, shards(): gathered = lax.all_gather(payload, 'y')  13.1 us
    all_gather x1, waiting for transfers between devices, shards(): all_kv = lax.all_gather(key_value, 'z', axis=0, tiled=True)  12.7 us
    pallas_call x1, Pallas kernels, shards(): pl.pallas_call(linear_kernel, out_shape=(shape((length, LANES), BF16), sh...  8.42 us
    all_to_all x1, waiting for transfers between devices, shards(): lax.all_to_all(partial, 'y', split_axis=0, concat_axis=0, tiled=True)  7.61 us
  transfers between devices with their start and end apart: 3, of which 2 were waited for; matrix products, arithmetic and copies ran while one was open for 2% of the time, Pallas kernels for 6%

profile of v4, /device:TPU:480, one launch (start us, length us, event | category | flops | bytes accessed | tf_op | source)
XLA Modules:
  0.0 159.9 jit_solution(17509503417098378710)
XLA Ops:
  6.5 0.0 copy-start.9
  6.5 0.0 copy-start.10
  6.5 0.0 copy-start.15
  6.5 0.0 copy-start.16
  6.5 0.0 copy-start.14
  6.5 0.0 copy-start.6
  6.6 0.0 copy-start.7
  6.6 0.0 copy-start.8
  6.6 0.0 copy-start.12
  6.6 0.0 copy-start.13
  6.6 0.0 all-gather.5.cloned.1.call-start
  6.6 13.5 %all-gather = bf16[128,2048]{1,0:T(8,128)(2,1)S(1)} all-gather(bf16[32,2048]{1,0:T(8,128)(2,1)} %param.22), channel_id=2, replica_groups=mesh['z'=16,'y'=4,'x'=4,'c'=2] {'x'}, dimensions={0}, use_global_device_ids=true | all-gather | bytes 655360 | tf_op jit(solution)/shard_map/all_gather | solution.py:409
  20.1 0.0 copy-start.17
  20.1 1.9 %collective-permute-start = (bf16[4,32,2048]{2,1,0:T(8,128)(2,1)S(1)}, bf16[4,32,2048]{2,1,0:T(8,128)(2,1)}, u32[]{:S(2)}, u32[]{:S(2)}) collective-permute-start(bf16[4,32,2048]{2,1,0:T(8,128)(2,1)S(1)} %bitcast.23), channel_id=1, source_target_pairs={{0,1},{1,0},{2,3},{3,2},{4,5},{5,4},{6,7},{7,6},{8,9},{9,8},{10,11... | collective-permute-start | bytes 1572872 | tf_op jit(solution)/shard_map/ppermute | solution.py:377
  22.0 0.7 tile.4
  22.7 0.7 reshape_tile.6.qg_ref
  23.4 0.7 tile.5
  24.0 0.6 reshape_tile.7.kg_ref
  24.6 0.0 collective-permute-done.other_ref
  24.6 0.0 copy-done.17
  24.6 4.0 %qkv.1 = (bf16[256,2048]{1,0:T(8,128)(2,1)}, bf16[256,128]{1,0:T(8,128)(2,1)}, bf16[256,256]{1,0:T(8,128)(2,1)}) custom-call(bf16[4,32,2048]{2,1,0:T(8,128)(2,1)} %bitcast.24, bf16[4,32,2048]{2,1,0:T(8,128)(2,1)} %collective-permute-done.other_ref, f32[1,2048]{1,0:T(1,128)} %bitcast.25, bf16[2048,128]{1,0:T(8,128)(2,1)} %wq_ref.1, bf16[2048,128]{1,0:T(8,128)(2,1)} %wk_ref.2, ...), custom_call_target="tpu_custom_call" | custom-call | flops 402653184 | bytes 6291456 | tf_op jit(solution)/shard_map/qkv/pallas_call | solution.py:411
  28.6 0.0 all-gather.5.cloned.1.call-update
  28.6 0.0 copy-done.9
  28.6 0.0 copy-done.10
  28.6 0.0 copy-done.15
  28.7 0.0 copy-done.16
  28.7 0.0 copy-done.14
  28.7 0.0 copy-done.6
  28.7 0.0 copy-done.7
  28.7 0.0 copy-done.8
  28.7 0.0 copy-done.12
  28.7 0.0 copy-done.13
  28.7 0.0 copy-start.5
  28.7 1.2 copy-done.5
  30.0 0.0 copy-start.11
  30.0 0.8 copy-done.11
  30.8 8.4 %linear.1 = (bf16[256,128]{1,0:T(8,128)(2,1)S(1)}, f32[256,128]{1,0:T(8,128)S(1)}, bf16[384,128]{1,0:T(8,128)(2,1)S(1)}) custom-call(bf16[256,2048]{1,0:T(8,128)(2,1)S(1)} %copy-done.5, bf16[256,128]{1,0:T(8,128)(2,1)S(1)} %copy-done.11, bf16[2048,128]{1,0:T(8,128)(2,1)S(1)} %copy-done.6, bf16[2048,128]{1,0:T(8,128)(2,1)S(1)} %copy-done.7, ...), custom_call_target="tpu_custom_call" | custom-call | flops 1073741824 | bytes 6291456 | tf_op jit(solution)/shard_map/linear/pallas_call | solution.py:434
  39.2 13.1 %all-gather.1 = bf16[1536,128]{1,0:T(8,128)(2,1)S(1)} all-gather(bf16[384,128]{1,0:T(8,128)(2,1)S(1)} %get-tuple-element.17), channel_id=3, replica_groups=mesh['z'=16,'y'=4,'x'=4,'c'=2] {'y'}, dimensions={0}, use_global_device_ids=true | all-gather | bytes 491520 | tf_op jit(solution)/shard_map/all_gather | solution.py:460
  52.3 0.0 copy-start.2
  52.3 0.5 row.1
  52.9 33.0 %all-gather.2 = bf16[2048,128]{1,0:T(8,128)(2,1)S(1)} all-gather(bf16[128,128]{1,0:T(8,128)(2,1)S(1)} %get-tuple-element.19), channel_id=4, replica_groups=mesh['z'=16,'y'=4,'x'=4,'c'=2] {'z'}, dimensions={0}, use_global_device_ids=true | all-gather | bytes 557056 | tf_op jit(solution)/shard_map/all_gather | solution.py:470
  85.8 1.1 carry.1.state_ref
  86.9 0.0 copy-start
  86.9 0.0 copy-start.1
  86.9 0.0 copy-start.3
  87.0 0.0 copy-start.4
  87.0 12.7 %all-gather.5.cloned.1.call-done.kv_hbm = bf16[4096,256]{1,0:T(8,128)(2,1)} async-done(((bf16[256,256]{1,0:T(8,128)(2,1)}), bf16[4096,256]{1,0:T(8,128)(2,1)}) %all-gather.5.cloned.1.call-update) | async-done | bytes 2097168 | tf_op jit(solution)/shard_map/all_gather | solution.py:433
  99.7 0.0 copy-done.2
  99.7 16.5 %attend.1 = bf16[4,272,256]{2,1,0:T(8,128)(2,1)} custom-call(bf16[4,384,128]{2,1,0:T(8,128)(2,1)} %bitcast.15, bf16[4096,256]{1,0:T(8,128)(2,1)} %all-gather.5.cloned.1.call-done.kv_hbm), custom_call_target="tpu_custom_call" | custom-call | flops 6442450944 | bytes 6291456 | tf_op jit(solution)/shard_map/attend/pallas_call | solution.py:482
  116.2 4.6 %all-to-all-start = ((bf16[4,272,256]{2,1,0:T(8,128)(2,1)}), bf16[4,272,256]{2,1,0:T(8,128)(2,1)S(1)}, u32[]{:S(2)}, u32[]{:S(2)}) async-start(bf16[4,272,256]{2,1,0:T(8,128)(2,1)} %attend.1), calls=%async_computation | async-start | bytes 1114112 | tf_op jit(solution)/shard_map/all_to_all | solution.py:498
  121.5 7.6 %all-to-all-done.parts_ref = bf16[4,272,256]{2,1,0:T(8,128)(2,1)S(1)} async-done(((bf16[4,272,256]{2,1,0:T(8,128)(2,1)}), bf16[4,272,256]{2,1,0:T(8,128)(2,1)S(1)}, u32[]{:S(2)}, u32[]{:S(2)}) %all-to-all-start) | async-done | bytes 557088 | tf_op jit(solution)/shard_map/all_to_all | solution.py:498
  129.1 0.0 copy-done
  129.1 0.0 copy-done.1
  129.1 0.0 copy-done.3
  129.1 0.0 copy-done.4
  129.1 2.5 %finish.1 = bf16[256,2048]{1,0:T(8,128)(2,1)S(1)} custom-call(f32[1]{0:T(128)S(6)} %copy.23.lam_ref, bf16[4,272,256]{2,1,0:T(8,128)(2,1)S(1)} %all-to-all-done.parts_ref, f32[1,128]{1,0:T(1,128)S(1)} %bitcast.16, bf16[256,128]{1,0:T(8,128)(2,1)S(1)} %get-tuple-element.22.qh_ref, f32[256,128]{1,0:T(8,128)S(1)} %get-tuple-element.23.ol_ref, ...), custom_call_target="tpu_custom_call" | custom-call | flops 268435456 | bytes 4194304 | tf_op jit(solution)/shard_map/finish/pallas_call | solution.py:499
  131.6 20.6 %all_to_all.10 = bf16[8,32,2048]{2,1,0:T(8,128)(2,1)S(1)} all-to-all(bf16[8,32,2048]{2,1,0:T(8,128)(2,1)S(1)} %bitcast.12), channel_id=1, replica_groups=mesh['z'=16,'y'=4,'x'=4,'c'=2] {'x','c'}, dimensions={0} | all-to-all | bytes 2097152 | tf_op jit(solution)/shard_map/all_to_all | solution.py:518
  152.2 0.8 reduce_sum.12
Async XLA Ops:
  6.5 22.1 %copy-start.9 = (bf16[2048,64]{0,1:T(8,128)(2,1)S(1)}, bf16[2048,64]{0,1:T(8,128)(2,1)}, u32[]{:S(2)}) copy-start(bf16[2048,64]{0,1:T(8,128)(2,1)} %param.27) | copy-start | bytes 786436
  6.5 22.1 %copy-start.10 = (bf16[2048,64]{0,1:T(8,128)(2,1)S(1)}, bf16[2048,64]{0,1:T(8,128)(2,1)}, u32[]{:S(2)}) copy-start(bf16[2048,64]{0,1:T(8,128)(2,1)} %param.28) | copy-start | bytes 786436
  6.5 22.1 %copy-start.15 = (f32[128]{0:T(128)S(1)}, f32[128]{0:T(128)}, u32[]{:S(2)}) copy-start(f32[128]{0:T(128)} %param.31) | copy-start | bytes 1540
  6.5 22.1 %copy-start.16 = (f32[128]{0:T(128)S(1)}, f32[128]{0:T(128)}, u32[]{:S(2)}) copy-start(f32[128]{0:T(128)} %param.32) | copy-start | bytes 1540
  6.5 22.1 %copy-start.14 = (f32[256,2]{0,1:T(2,128)S(1)}, f32[256,2]{0,1:T(2,128)}, u32[]{:S(2)}) copy-start(f32[256,2]{0,1:T(2,128)} %param.33) | copy-start | bytes 6148
  6.5 22.1 %copy-start.6 = (bf16[2048,128]{1,0:T(8,128)(2,1)S(1)}, bf16[2048,128]{1,0:T(8,128)(2,1)}, u32[]{:S(2)}) copy-start(bf16[2048,128]{1,0:T(8,128)(2,1)} %wr_ref.1) | copy-start | bytes 1572868
  6.6 22.1 %copy-start.7 = (bf16[2048,128]{1,0:T(8,128)(2,1)S(1)}, bf16[2048,128]{1,0:T(8,128)(2,1)}, u32[]{:S(2)}) copy-start(bf16[2048,128]{1,0:T(8,128)(2,1)} %wk_ref.3) | copy-start | bytes 1572868
  6.6 22.1 %copy-start.8 = (bf16[2048,128]{1,0:T(8,128)(2,1)S(1)}, bf16[2048,128]{1,0:T(8,128)(2,1)}, u32[]{:S(2)}) copy-start(bf16[2048,128]{1,0:T(8,128)(2,1)} %wv_ref.3) | copy-start | bytes 1572868
  6.6 22.1 %copy-start.12 = (bf16[64,128]{1,0:T(8,128)(2,1)S(1)}, bf16[64,128]{1,0:T(8,128)(2,1)}, u32[]{:S(2)}) copy-start(bf16[64,128]{1,0:T(8,128)(2,1)} %du_ref.1) | copy-start | bytes 49156
  6.6 22.1 %copy-start.13 = (bf16[64,128]{1,0:T(8,128)(2,1)S(1)}, bf16[64,128]{1,0:T(8,128)(2,1)}, u32[]{:S(2)}) copy-start(bf16[64,128]{1,0:T(8,128)(2,1)} %ru_ref.1) | copy-start | bytes 49156
  6.6 93.1 %all-gather.5.cloned.1.call-start = ((), (), s32[]{:S(2)}) async-start(), calls=%async_computation.2 | async-start | bytes 2228224 | tf_op jit(solution)/shard_map/all_gather | solution.py:433
  20.1 4.5 %copy-start.17 = (bf16[128,2048]{1,0:T(8,128)(2,1)}, bf16[128,2048]{1,0:T(8,128)(2,1)S(1)}, u32[]{:S(2)}) copy-start(bf16[128,2048]{1,0:T(8,128)(2,1)S(1)} %all-gather) | copy-start | bytes 1572868
  20.1 4.5 %collective-permute-start = (bf16[4,32,2048]{2,1,0:T(8,128)(2,1)S(1)}, bf16[4,32,2048]{2,1,0:T(8,128)(2,1)}, u32[]{:S(2)}, u32[]{:S(2)}) collective-permute-start(bf16[4,32,2048]{2,1,0:T(8,128)(2,1)S(1)} %bitcast.23), channel_id=1, source_target_pairs={{0,1},{1,0},{2,3},{3,2},{4,5},{5,4},{6,7},{7,6},{8,9},{9,8},{10,11... | collective-permute-start | bytes 1572872 | tf_op jit(solution)/shard_map/ppermute | solution.py:377
  28.7 1.2 copy-start.5
  30.0 0.8 copy-start.11
  52.3 47.4 %copy-start.2 = (bf16[1536,128]{1,0:T(8,128)(2,1)}, bf16[1536,128]{1,0:T(8,128)(2,1)S(1)}, u32[]{:S(2)}) copy-start(bf16[1536,128]{1,0:T(8,128)(2,1)S(1)} %all-gather.1) | copy-start | bytes 1179652
  86.9 42.1 %copy-start = (bf16[128,2048]{1,0:T(8,128)(2,1)S(1)}, bf16[128,2048]{1,0:T(8,128)(2,1)}, u32[]{:S(2)}) copy-start(bf16[128,2048]{1,0:T(8,128)(2,1)} %wl_ref.1) | copy-start | bytes 1572868
  86.9 42.1 %copy-start.1 = (bf16[128,2048]{1,0:T(8,128)(2,1)S(1)}, bf16[128,2048]{1,0:T(8,128)(2,1)}, u32[]{:S(2)}) copy-start(bf16[128,2048]{1,0:T(8,128)(2,1)} %wa_ref.1) | copy-start | bytes 1572868
  86.9 42.1 %copy-start.3 = (f32[128]{0:T(128)S(1)}, f32[128]{0:T(128)}, u32[]{:S(2)}) copy-start(f32[128]{0:T(128)} %param.41) | copy-start | bytes 1540
  87.0 42.1 %copy-start.4 = (f32[128]{0:T(128)S(1)}, f32[128]{0:T(128)}, u32[]{:S(2)}) copy-start(f32[128]{0:T(128)} %param.34) | copy-start | bytes 1540
  116.2 12.9 %all-to-all-start = ((bf16[4,272,256]{2,1,0:T(8,128)(2,1)}), bf16[4,272,256]{2,1,0:T(8,128)(2,1)S(1)}, u32[]{:S(2)}, u32[]{:S(2)}) async-start(bf16[4,272,256]{2,1,0:T(8,128)(2,1)} %attend.1), calls=%async_computation | async-start | bytes 1114112 | tf_op jit(solution)/shard_map/all_to_all | solution.py:498
Sparse Core Ops, SparseCore 0:
  28.7 70.8 all-gather.4
